TPU v7x, 256 devices: a whole 4x4x8 slice. The times are simulated.
256 devices in a mesh: sp: 32 (over z, y), fs: 4 (over x), tp: 2 (over core).
Axes of the slice: x: 4, y: 4, z: 8, core: 2. Of those that a mesh axis runs over, the one named last changes fastest.
Arguments:
- tokens: bfloat16 [16384, 2048], P('sp', ('fs', 'tp')), may hold values from -6 to 6
- in_gain: float32 [2048], replicated, may hold values from 0.1 to 1.9
- conv_a_weight: bfloat16 [2048, 1024], P(None, ('fs', 'tp')), may hold values from -0.125 to 0.125
- conv_gate_weight: bfloat16 [2048, 1024], P(None, ('fs', 'tp')), may hold values from -0.125 to 0.125
- query_weight: bfloat16 [2048, 1024], P(None, ('fs', 'tp')), may hold values from -0.125 to 0.125
- key_weight: bfloat16 [2048, 1024], P(None, ('fs', 'tp')), may hold values from -0.125 to 0.125
- value_weight: bfloat16 [2048, 1024], P(None, ('fs', 'tp')), may hold values from -0.125 to 0.125
- conv_taps: bfloat16 [31, 1024], replicated, may hold values from -3 to 3
- conv_norm_gain: float32 [1024], replicated, may hold values from 0.1 to 1.9
- break_shift: bfloat16 [16, 16384], P(('fs', 'tp'), 'sp'), may hold values from -20 to 1
- conv_out_gain: float32 [1024], replicated, may hold values from 0.1 to 1.9
- attn_out_gain: float32 [1024], replicated, may hold values from 0.1 to 1.9
- out_weight: bfloat16 [2048, 2048], P(None, ('fs', 'tp')), may hold values from -0.125 to 0.125
Outputs:
- mixed: bfloat16 [16384, 2048], P('sp', ('fs', 'tp'))
All inputs are finite; a program needn't handle non-finite values.
Results may differ from a plain program's by a relative error of at most 0.0078.
Values may be sent and summed in bfloat16 or wider, within the bound.
A program may use at most 128 MiB of HBM per device.

v0:
```python
import jax
import jax.numpy as jnp
from jax import lax
from jax.sharding import PartitionSpec as P

HEAD_DIM = 64


epsilon = 1e-06


def from_everyone(shard, axis):
    copies = jnp.broadcast_to(shard, (lax.axis_size(axis), *shard.shape))
    return lax.all_to_all(copies, axis, split_axis=0, concat_axis=0, tiled=True)


def laid_out(parts, dim):
    dims = list(parts.shape[1:])
    dims[dim] *= parts.shape[0]
    return jnp.moveaxis(parts, 0, dim).reshape(dims)


def gather_directly(shard, axis, dim):
    parts = from_everyone(shard, axis)
    return laid_out(parts, dim)


def passed_along(shard, axis, by):
    count = lax.axis_size(axis)
    pairs = [(i, i + by) for i in range(count) if 0 <= i + by < count]
    return lax.ppermute(shard, axis, pairs)


def over_copies(shard, axis):
    everything = from_everyone(shard, axis)
    return jnp.sum(everything, axis=0)


def packed_total(arrays, axis):
    line, at, finished = (jnp.concatenate([a.reshape(-1) for a in arrays]), 0, [])
    so_far = over_copies(line, axis)
    for a in arrays:
        finished.append(so_far[at : at + a.size].reshape(a.shape))
        at += a.size
    return tuple(finished)


def rows_first(arrays, axis, dims):
    turned = [jnp.moveaxis(a, dim, 0) for a, dim in zip(arrays, dims)]
    widths = [t[0].size for t in turned]
    both = jnp.concatenate([t.reshape(-1, w) for t, w in zip(turned, widths)], axis=1)
    out = lax.all_gather(both, axis, axis=0, tiled=True)
    parts = jnp.split(out, [sum(widths[:k]) for k in range(1, len(widths))], axis=1)
    return tuple(
        (
            jnp.moveaxis(b.reshape(-1, *t.shape[1:]), 0, dim)
            for b, t, dim in zip(parts, turned, dims)
        )
    )


def piece_ends(length, count):
    unit = 8 if length >= 8 * count else 1
    return [length // unit * k // count * unit for k in range(1, count)]


def gather_in_order(shard, axes, order):
    parts = shard
    for k in order:
        parts = lax.all_gather(parts, axes[k])
    done = order[::-1]
    back = [done.index(k) for k in range(len(axes))]
    parts = parts.transpose(*back, *range(len(axes), parts.ndim))
    return parts.reshape(-1, *shard.shape)


def spread_gather(shard, axes, dim):
    widest = max(range(max(1, shard.ndim - 1)), key=lambda d: shard.shape[d])
    count, finished = (len(axes), [])
    for first, piece in enumerate(
        jnp.split(shard, piece_ends(shard.shape[widest], count), axis=widest)
    ):
        if piece.size:
            order = [(first - k) % count for k in range(count)]
            finished.append(gather_in_order(piece, axes, order))
    return laid_out(jnp.concatenate(finished, axis=widest + 1), dim)


def per_device(
    tokens,
    in_gain,
    conv_a_weight,
    conv_gate_weight,
    query_weight,
    key_weight,
    value_weight,
    conv_taps,
    conv_norm_gain,
    break_shift,
    conv_out_gain,
    attn_out_gain,
    out_weight,
):
    rows_here = tokens.shape[0]
    model_width = in_gain.shape[0]
    channels = model_width // 2
    local_width = conv_a_weight.shape[1]
    heads_here = break_shift.shape[0]
    group_index = lax.axis_index(("fs", "tp"))
    shard_index = lax.axis_index("sp")
    stacked = jnp.concatenate(
        (conv_a_weight, conv_gate_weight, query_weight, key_weight, value_weight), axis=1
    )
    segment = gather_directly(tokens, ("fs", "tp"), 1)
    segment_wide = segment.astype(jnp.float32)
    scaled = (segment_wide * in_gain[None, :]).astype(jnp.bfloat16)
    totals = jnp.dot(scaled, stacked, preferred_element_type=jnp.float32)
    totals, squares = (totals, jnp.sum(segment_wide * segment_wide, axis=1))
    input_scale = lax.rsqrt(squares / model_width + epsilon)
    projected = (totals * input_scale[:, None]).astype(jnp.bfloat16)
    conv_a = projected[:, :local_width]
    conv_gate = projected[:, local_width : 2 * local_width]
    query = projected[:, 2 * local_width : 3 * local_width]
    key = projected[:, 3 * local_width : 4 * local_width]
    value = projected[:, 4 * local_width :]
    gated_input = conv_a.astype(jnp.float32) * jax.nn.sigmoid(conv_gate.astype(jnp.float32))
    reach_rows = conv_taps.shape[0] - 1
    earlier = passed_along(gated_input[rows_here - reach_rows :], "sp", 1)
    padded = jnp.concatenate((earlier, gated_input), axis=0)
    tap_values = lax.dynamic_slice_in_dim(
        conv_taps, group_index * local_width, local_width, 1
    ).astype(jnp.float32)
    conv_out = jnp.zeros((rows_here, local_width), jnp.float32)
    for offset in range(reach_rows + 1):
        conv_out = conv_out + tap_values[offset][None, :] * padded[offset : offset + rows_here]
    first_sum, second_sum = packed_total(
        (jnp.sum(conv_out, axis=1), jnp.sum(conv_out * conv_out, axis=1)), ("fs", "tp")
    )
    row_mean = first_sum / channels
    row_spread = second_sum / channels - row_mean * row_mean
    centered = conv_out - row_mean[:, None]
    norm_gain = lax.dynamic_slice_in_dim(conv_norm_gain, group_index * local_width, local_width, 0)
    normed = centered * lax.rsqrt(row_spread + epsilon)[:, None] * norm_gain[None, :]
    conv_mixed = jax.nn.silu(normed).astype(jnp.bfloat16)
    queries = query.reshape(rows_here, heads_here, HEAD_DIM)
    query_pos = shard_index * rows_here + jnp.arange(rows_here, dtype=jnp.int32)
    score_scale = HEAD_DIM ** (-0.5)

    def attend(running, key_rows, value_rows, shift_rows, start_pos):
        outputs, behind = running
        piece_rows = key_rows.shape[0]
        key_heads = key_rows.reshape(piece_rows, heads_here, HEAD_DIM)
        value_heads = value_rows.reshape(piece_rows, heads_here, HEAD_DIM)
        scores = (
            jnp.einsum("qhd,khd->hqk", queries, key_heads, preferred_element_type=jnp.float32)
            * score_scale
        )
        scores = scores + shift_rows.astype(jnp.float32)[:, None, :]
        key_pos = start_pos + jnp.arange(piece_rows, dtype=jnp.int32)
        allowed = ((key_pos[None, :] < query_pos[:, None]) & (key_pos[None, :] >= 0))[None]
        log_fail = jnp.where(allowed, jax.nn.log_sigmoid(-scores), 0.0)
        later_sum = lax.cumsum(log_fail, axis=2, reverse=True) - log_fail + behind[:, :, None]
        weights = jnp.where(allowed, jnp.exp(jax.nn.log_sigmoid(scores) + later_sum), 0.0).astype(
            jnp.bfloat16
        )
        outputs = outputs + jnp.einsum(
            "hqk,khd->qhd", weights, value_heads, preferred_element_type=jnp.float32
        )
        return (outputs, behind + jnp.sum(log_fail, axis=2))

    start_state = (
        jnp.zeros((rows_here, heads_here, HEAD_DIM), jnp.float32),
        jnp.zeros((heads_here, rows_here), jnp.float32),
    )
    all_keys, all_values, all_shifts = rows_first((key, value, break_shift), "sp", (0, 0, 1))
    sp_count = lax.axis_size("sp")
    grouped = 1
    while grouped * 2 * rows_here <= 1024 and sp_count % (grouped * 2) == 0:
        grouped = grouped * 2
    block_rows = grouped * rows_here
    last_block = (shard_index * rows_here + rows_here - 1) // block_rows

    def advance(counter, running):
        begin_row = (last_block - counter) * block_rows
        key_rows = lax.dynamic_slice_in_dim(all_keys, begin_row, block_rows, 0)
        value_rows = lax.dynamic_slice_in_dim(all_values, begin_row, block_rows, 0)
        shift_rows = lax.dynamic_slice_in_dim(all_shifts, begin_row, block_rows, 1)
        return attend(running, key_rows, value_rows, shift_rows, begin_row)

    outputs, behind = lax.fori_loop(0, last_block + 1, advance, start_state)
    attn_mixed = outputs.reshape(rows_here, heads_here * HEAD_DIM).astype(jnp.bfloat16)
    conv_piece = spread_gather(conv_mixed, ("fs", "tp"), 1)
    attn_piece = spread_gather(attn_mixed, ("fs", "tp"), 1)
    piece_width = conv_piece.shape[1]
    conv_wide = conv_piece.astype(jnp.float32)
    attn_wide = attn_piece.astype(jnp.float32)
    conv_scaled = (conv_wide * conv_out_gain[None, :]).astype(jnp.bfloat16)
    attn_scaled = (attn_wide * attn_out_gain[None, :]).astype(jnp.bfloat16)
    conv_rows = lax.slice_in_dim(out_weight, 0, piece_width, axis=0)
    attn_rows = lax.dynamic_slice_in_dim(out_weight, channels, piece_width, 0)
    conv_total = jnp.dot(conv_scaled, conv_rows, preferred_element_type=jnp.float32)
    attn_total = jnp.dot(attn_scaled, attn_rows, preferred_element_type=jnp.float32)
    conv_squares = jnp.sum(conv_wide * conv_wide, axis=1)
    attn_squares = jnp.sum(attn_wide * attn_wide, axis=1)
    conv_total, attn_total, conv_squares, attn_squares = (
        conv_total,
        attn_total,
        conv_squares,
        attn_squares,
    )
    conv_scale = lax.rsqrt(conv_squares / channels + epsilon)
    attn_scale = lax.rsqrt(attn_squares / channels + epsilon)
    mixed = conv_total * conv_scale[:, None] + attn_total * attn_scale[:, None]
    return mixed.astype(jnp.bfloat16)


def solution(mesh):
    return jax.shard_map(
        per_device,
        mesh=mesh,
        in_specs=(
            P("sp", ("fs", "tp")),
            P(),
            P(None, ("fs", "tp")),
            P(None, ("fs", "tp")),
            P(None, ("fs", "tp")),
            P(None, ("fs", "tp")),
            P(None, ("fs", "tp")),
            P(),
            P(),
            P(("fs", "tp"), "sp"),
            P(),
            P(),
            P(None, ("fs", "tp")),
        ),
        out_specs=P("sp", ("fs", "tp")),
        check_vma=False,
    )
```

profile of v0, /device:TPU:243, one launch (start us, length us, event | category | flops | bytes accessed | tf_op | source)
XLA Modules:
  0.0 726.8 jit_solution(10519590968202718702)
XLA Ops:
  9.2 5.1 all-to-all-start
  21.0 18.5 %all-to-all-done = bf16[8,512,256]{1,2,0:T(8,128)(2,1)S(1)} async-done(((bf16[8,512,256]{1,2,0:T(8,128)(2,1)}), bf16[8,512,256]{1,2,0:T(8,128)(2,1)S(1)}, u32[]{:S(2)}, u32[]{:S(2)}) %all-to-all-start) | async-done | bytes 2097184 | tf_op jit(solution)/shard_map/all_to_all | solution.py:14
  40.5 3.6 fusion.21
  52.0 6.4 all-to-all-start.1
  64.7 10.0 %all-gather.3 = bf16[8,256,128]{2,1,0:T(8,128)(2,1)S(1)} all-gather(bf16[2,256,128]{2,1,0:T(8,128)(2,1)S(1)} %bitcast.176), channel_id=5, replica_groups=mesh['sp'=32,'fs'=4,'tp'=2] {'fs'}, dimensions={0}, use_global_device_ids=true | all-gather | bytes 655360 | tf_op jit(solution)/shard_map/all_gather | solution.py:70
  74.9 10.2 %all-gather = bf16[1024,128]{1,0:T(8,128)(2,1)S(1)} all-gather(bf16[256,128]{1,0:T(8,128)(2,1)S(1)} %get-tuple-element.173), channel_id=2, replica_groups=mesh['sp'=32,'fs'=4,'tp'=2] {'fs'}, dimensions={0}, use_global_device_ids=true | all-gather | bytes 327680 | tf_op jit(solution)/shard_map/all_gather | solution.py:70
  85.1 6.4 all-gather.1
  92.5 67.0 %all-gather.8.cloned.1.call-done = bf16[16384,258]{1,0:T(8,128)(2,1)} async-done(((bf16[512,258]{1,0:T(8,128)(2,1)}), bf16[16384,258]{1,0:T(8,128)(2,1)}) %all-gather.8.cloned.1.call-update) | async-done | bytes 8454160 | tf_op jit(solution)/shard_map/all_gather | solution.py:52
  159.5 3.7 slice_bitcast_fusion.1
  163.2 3.7 copy.91
  167.0 5.8 fusion.117
  172.8 512.7 %while.13 = (s32[]{:T(128)}, f32[512,2,64]{0,2,1:T(8,128)S(1)}, f32[2,512]{1,0:T(2,128)S(1)}, s32[]{:T(128)}, s32[]{:T(128)}, /*index=5*/bf16[16384,128]{1,0:T(8...) while((s32[]{:T(128)}, f32[512,2,64]{0,2,1:T(8,128)S(1)}, ...), condition=%wide.region_9.10_spmd.clone, body=%wide.region_5.9_spmd.clone.sunk | while | flops 439489024 | bytes 84838688 | solution.py:190
  175.3 5.1 fusion.142
  180.3 10.1 %fusion.143 = f32[2,512,8,128]{1,2,3,0:T(8,128)S(1)} fusion(f32[2,512,8,128]{1,3,2,0:T(8,128)S(1)} %bitcast.166), kind=kOutput, calls=%fused_computation.19.clone.1 | output fusion | flops 133169152 | bytes 8388608 | tf_op jit(solution)/shard_map/reduce-window
  197.6 6.9 fusion.144
  207.3 5.0 fusion.142
  212.3 10.1 %fusion.143 = f32[2,512,8,128]{1,2,3,0:T(8,128)S(1)} fusion(f32[2,512,8,128]{1,3,2,0:T(8,128)S(1)} %bitcast.166), kind=kOutput, calls=%fused_computation.19.clone.1 | output fusion | flops 133169152 | bytes 8388608 | tf_op jit(solution)/shard_map/reduce-window
  229.6 6.9 fusion.144
  239.3 5.1 fusion.142
  244.4 10.1 %fusion.143 = f32[2,512,8,128]{1,2,3,0:T(8,128)S(1)} fusion(f32[2,512,8,128]{1,3,2,0:T(8,128)S(1)} %bitcast.166), kind=kOutput, calls=%fused_computation.19.clone.1 | output fusion | flops 133169152 | bytes 8388608 | tf_op jit(solution)/shard_map/reduce-window
  261.7 6.9 fusion.144
  271.4 5.1 fusion.142
  276.4 10.1 %fusion.143 = f32[2,512,8,128]{1,2,3,0:T(8,128)S(1)} fusion(f32[2,512,8,128]{1,3,2,0:T(8,128)S(1)} %bitcast.166), kind=kOutput, calls=%fused_computation.19.clone.1 | output fusion | flops 133169152 | bytes 8388608 | tf_op jit(solution)/shard_map/reduce-window
  293.7 6.9 fusion.144
  303.4 5.1 fusion.142
  308.4 10.1 %fusion.143 = f32[2,512,8,128]{1,2,3,0:T(8,128)S(1)} fusion(f32[2,512,8,128]{1,3,2,0:T(8,128)S(1)} %bitcast.166), kind=kOutput, calls=%fused_computation.19.clone.1 | output fusion | flops 133169152 | bytes 8388608 | tf_op jit(solution)/shard_map/reduce-window
  325.7 6.9 fusion.144
  335.4 5.0 fusion.142
  340.5 10.1 %fusion.143 = f32[2,512,8,128]{1,2,3,0:T(8,128)S(1)} fusion(f32[2,512,8,128]{1,3,2,0:T(8,128)S(1)} %bitcast.166), kind=kOutput, calls=%fused_computation.19.clone.1 | output fusion | flops 133169152 | bytes 8388608 | tf_op jit(solution)/shard_map/reduce-window
  357.8 6.9 fusion.144
  367.5 5.1 fusion.142
  372.5 10.1 %fusion.143 = f32[2,512,8,128]{1,2,3,0:T(8,128)S(1)} fusion(f32[2,512,8,128]{1,3,2,0:T(8,128)S(1)} %bitcast.166), kind=kOutput, calls=%fused_computation.19.clone.1 | output fusion | flops 133169152 | bytes 8388608 | tf_op jit(solution)/shard_map/reduce-window
  389.8 6.9 fusion.144
  399.5 5.0 fusion.142
  404.5 10.1 %fusion.143 = f32[2,512,8,128]{1,2,3,0:T(8,128)S(1)} fusion(f32[2,512,8,128]{1,3,2,0:T(8,128)S(1)} %bitcast.166), kind=kOutput, calls=%fused_computation.19.clone.1 | output fusion | flops 133169152 | bytes 8388608 | tf_op jit(solution)/shard_map/reduce-window
  421.8 6.9 fusion.144
  431.5 5.1 fusion.142
  436.6 10.1 %fusion.143 = f32[2,512,8,128]{1,2,3,0:T(8,128)S(1)} fusion(f32[2,512,8,128]{1,3,2,0:T(8,128)S(1)} %bitcast.166), kind=kOutput, calls=%fused_computation.19.clone.1 | output fusion | flops 133169152 | bytes 8388608 | tf_op jit(solution)/shard_map/reduce-window
  453.9 6.9 fusion.144
  463.6 5.1 fusion.142
  468.6 10.1 %fusion.143 = f32[2,512,8,128]{1,2,3,0:T(8,128)S(1)} fusion(f32[2,512,8,128]{1,3,2,0:T(8,128)S(1)} %bitcast.166), kind=kOutput, calls=%fused_computation.19.clone.1 | output fusion | flops 133169152 | bytes 8388608 | tf_op jit(solution)/shard_map/reduce-window
  485.9 6.9 fusion.144
  495.6 5.1 fusion.142
  500.6 10.1 %fusion.143 = f32[2,512,8,128]{1,2,3,0:T(8,128)S(1)} fusion(f32[2,512,8,128]{1,3,2,0:T(8,128)S(1)} %bitcast.166), kind=kOutput, calls=%fused_computation.19.clone.1 | output fusion | flops 133169152 | bytes 8388608 | tf_op jit(solution)/shard_map/reduce-window
  517.9 6.9 fusion.144
  527.6 5.0 fusion.142
  532.7 10.1 %fusion.143 = f32[2,512,8,128]{1,2,3,0:T(8,128)S(1)} fusion(f32[2,512,8,128]{1,3,2,0:T(8,128)S(1)} %bitcast.166), kind=kOutput, calls=%fused_computation.19.clone.1 | output fusion | flops 133169152 | bytes 8388608 | tf_op jit(solution)/shard_map/reduce-window
  550.0 6.9 fusion.144
  559.7 5.1 fusion.142
  564.7 10.1 %fusion.143 = f32[2,512,8,128]{1,2,3,0:T(8,128)S(1)} fusion(f32[2,512,8,128]{1,3,2,0:T(8,128)S(1)} %bitcast.166), kind=kOutput, calls=%fused_computation.19.clone.1 | output fusion | flops 133169152 | bytes 8388608 | tf_op jit(solution)/shard_map/reduce-window
  582.0 6.9 fusion.144
  591.7 5.0 fusion.142
  596.7 10.1 %fusion.143 = f32[2,512,8,128]{1,2,3,0:T(8,128)S(1)} fusion(f32[2,512,8,128]{1,3,2,0:T(8,128)S(1)} %bitcast.166), kind=kOutput, calls=%fused_computation.19.clone.1 | output fusion | flops 133169152 | bytes 8388608 | tf_op jit(solution)/shard_map/reduce-window
  614.0 6.9 fusion.144
  623.7 5.1 fusion.142
  628.8 10.1 %fusion.143 = f32[2,512,8,128]{1,2,3,0:T(8,128)S(1)} fusion(f32[2,512,8,128]{1,3,2,0:T(8,128)S(1)} %bitcast.166), kind=kOutput, calls=%fused_computation.19.clone.1 | output fusion | flops 133169152 | bytes 8388608 | tf_op jit(solution)/shard_map/reduce-window
  646.1 6.9 fusion.144
  655.8 5.1 fusion.142
  660.8 10.1 %fusion.143 = f32[2,512,8,128]{1,2,3,0:T(8,128)S(1)} fusion(f32[2,512,8,128]{1,3,2,0:T(8,128)S(1)} %bitcast.166), kind=kOutput, calls=%fused_computation.19.clone.1 | output fusion | flops 133169152 | bytes 8388608 | tf_op jit(solution)/shard_map/reduce-window
  678.1 6.9 fusion.144
  685.7 3.0 all_gather.65
  688.6 9.9 %all-gather.5 = bf16[8,256,128]{2,1,0:T(8,128)(2,1)S(1)} all-gather(bf16[2,256,128]{2,1,0:T(8,128)(2,1)S(1)} %all_gather.65), channel_id=7, replica_groups=mesh['sp'=32,'fs'=4,'tp'=2] {'fs'}, dimensions={0}, use_global_device_ids=true | all-gather | bytes 655360 | tf_op jit(solution)/shard_map/all_gather | solution.py:70
  698.9 9.4 %all_gather.61 = bf16[4,256,128]{2,1,0:T(8,128)(2,1)S(1)} all-gather(bf16[1,256,128]{2,1,0:T(8,128)(2,1)S(1)} %copy.92), channel_id=1, replica_groups=mesh['sp'=32,'fs'=4,'tp'=2] {'fs'}, dimensions={0}, use_global_device_ids=true | all-gather | bytes 327680 | tf_op jit(solution)/shard_map/all_gather | solution.py:70
  708.2 8.6 %all-gather.4 = bf16[8,256,128]{2,1,0:T(8,128)(2,1)S(1)} all-gather(bf16[4,256,128]{2,1,0:T(8,128)(2,1)S(1)} %all_gather.61), channel_id=6, replica_groups=mesh['sp'=32,'fs'=4,'tp'=2] {'tp'}, dimensions={0}, use_global_device_ids=true | all-gather | bytes 786432 | tf_op jit(solution)/shard_map/all_gather | solution.py:70
  (374 shorter events, 187.6 us)
Async XLA Ops:
  6.5 7.8 %copy-start.8 = (bf16[2,512]{1,0:T(2,128)(2,1)S(1)}, bf16[2,512]{1,0:T(2,128)(2,1)}, u32[]{:S(2)}) copy-start(bf16[2,512]{1,0:T(2,128)(2,1)} %param.24) | copy-start | bytes 6148
  6.5 8.0 %copy-start.2 = (bf16[2048,128]{1,0:T(8,128)(2,1)S(1)}, bf16[2048,128]{1,0:T(8,128)(2,1)}, u32[]{:S(2)}) copy-start(bf16[2048,128]{1,0:T(8,128)(2,1)} %param.17) | copy-start | bytes 1572868
  6.5 8.9 %copy-start.3 = (bf16[2048,128]{1,0:T(8,128)(2,1)S(1)}, bf16[2048,128]{1,0:T(8,128)(2,1)}, u32[]{:S(2)}) copy-start(bf16[2048,128]{1,0:T(8,128)(2,1)} %param.18) | copy-start | bytes 1572868
  9.2 30.2 %all-to-all-start = ((bf16[8,512,256]{1,2,0:T(8,128)(2,1)}), bf16[8,512,256]{1,2,0:T(8,128)(2,1)S(1)}, u32[]{:S(2)}, u32[]{:S(2)}) async-start(bf16[8,512,256]{1,2,0:T(8,128)(2,1)} %broadcast_in_dim.22), calls=%async_computation | async-start | bytes 4194304 | tf_op jit(solution)/shard_map/all_to_all | solution.py:14
  14.3 25.7 %copy-start.5 = (f32[2048]{0:T(1024)S(1)}, f32[2048]{0:T(1024)}, u32[]{:S(2)}) copy-start(f32[2048]{0:T(1024)} %param.16) | copy-start | bytes 24580
  14.3 145.2 %all-gather.8.cloned.1.call-start = ((), (), s32[]{:S(2)}) async-start(), calls=%async_computation.2 | async-start | bytes 12976128 | tf_op jit(solution)/shard_map/all_gather | solution.py:52
  14.5 5.6 copy-start.4
  45.7 4.5 collective-permute-start
  52.0 10.2 %all-to-all-start.1 = ((f32[8,1,1024]{2,1,0:T(1,128)}), f32[8,1,1024]{2,1,0:T(1,128)S(1)}, u32[]{:S(2)}, u32[]{:S(2)}) async-start(f32[8,1,1024]{2,1,0:T(1,128)} %broadcast_in_dim.29), calls=%async_computation.1 | async-start | bytes 65536 | tf_op jit(solution)/shard_map/all_to_all | solution.py:14
  62.4 29.8 %copy-start.6 = (f32[1024]{0:T(1024)S(1)}, f32[1024]{0:T(1024)}, u32[]{:S(2)}) copy-start(f32[1024]{0:T(1024)} %param.25) | copy-start | bytes 12292
  190.4 2.0 copy-start
  195.2 2.4 copy-start.1
  222.4 2.0 copy-start
  227.2 2.4 copy-start.1
  254.5 2.0 copy-start
  259.2 2.4 copy-start.1
  286.5 2.0 copy-start
  291.2 2.4 copy-start.1
  318.5 2.0 copy-start
  323.3 2.4 copy-start.1
  350.6 2.0 copy-start
  355.3 2.4 copy-start.1
  382.6 2.0 copy-start
  387.4 2.4 copy-start.1
  414.6 2.0 copy-start
  419.4 2.4 copy-start.1
  446.7 2.0 copy-start
  451.4 2.4 copy-start.1
  478.7 2.0 copy-start
  483.5 2.4 copy-start.1
  510.7 2.0 copy-start
  515.5 2.4 copy-start.1
  542.8 2.0 copy-start
  547.5 2.4 copy-start.1
  574.8 2.0 copy-start
  579.6 2.4 copy-start.1
  606.8 2.0 copy-start
  611.6 2.4 copy-start.1
  638.9 2.0 copy-start
  643.6 2.4 copy-start.1
  670.9 2.0 copy-start
  675.7 2.4 copy-start.1
  685.7 32.0 %copy-start.7 = (f32[1024]{0:T(1024)S(1)}, f32[1024]{0:T(1024)}, u32[]{:S(2)}) copy-start(f32[1024]{0:T(1024)} %param.26) | copy-start | bytes 12292
  717.1 1.2 copy-start.9
Sparse Core Ops, SparseCore 0:
  45.0 114.4 all-gather.7
where the time goes:
time: 728 us; the launch traced here: 727 us
  other arithmetic  335 us (46%)
  local copies, waits for them, and re-layouts  118 us (16%)
  matrix products  93.9 us (13%)
  waiting for transfers between devices  89.9 us (12%)
  blocking collectives  59.7 us (8%)
  starting transfers between devices  14.5 us (2%)
  between operations  13.7 us (2%)
    another operation x32, other arithmetic  162 us
    convert_element_type x16, other arithmetic, attend(): jnp.where(allowed, jnp.exp(jax.nn.log_sigmoid(scores) + later_sum), 0.0)  110 us
    dot_general x16, matrix products, attend(): jnp.einsum('qhd,khd->hqk', queries, key_heads, preferred_element_type=jnp...  80.8 us
    all_gather x1, waiting for transfers between devices, rows_first(): out = lax.all_gather(both, axis, axis=0, tiled=True)  67 us
    all_gather x8, blocking collectives, gather_in_order(): parts = lax.all_gather(parts, axes[k])  59.7 us
    another operation x16, other arithmetic, attend(): lax.cumsum(log_fail, axis=2, reverse=True) - log_fail + behind[:, :, None]  43.3 us
    another operation x16, local copies, waits for them, and re-layouts, attend(): lax.cumsum(log_fail, axis=2, reverse=True) - log_fail + behind[:, :, None]  38.9 us
    while x64, local copies, waits for them, and re-layouts  31.3 us
  transfers between devices with their start and end apart: 4, of which 4 were waited for; matrix products, arithmetic and copies ran while one was open for 2% of the time, Pallas kernels for 0%

commit v1 on v0

v1 whole, which is shorter than its diff:
```python
import jax
import jax.numpy as jnp
from jax import lax
from jax.experimental import pallas as pl
from jax.experimental.pallas import tpu as pltpu
from jax.sharding import PartitionSpec as P

MESH = pl.DeviceIdType.MESH
VMEM = pltpu.VMEM
HEAD = 64
PLANES, BLOCKS, RING, CORES = 8, 4, 4, 2
SHIFT_ROWS = 16
epsilon = 1e-06
f32, bf16 = jnp.float32, jnp.bfloat16


def position():
    return lax.axis_index("sp"), lax.axis_index("fs"), lax.axis_index("tp")


def greet(devices):
    barrier = pltpu.get_barrier_semaphore()
    for device in devices:
        pl.semaphore_signal(barrier, inc=1, device_id=device, device_id_type=MESH)
    pl.semaphore_wait(barrier, len(devices))


def remote(src, dst, send, recv, device):
    return pltpu.make_async_remote_copy(
        src_ref=src, dst_ref=dst, send_sem=send, recv_sem=recv, device_id=device, device_id_type=MESH
    )


def left_lanes(shape):
    return lax.broadcasted_iota(jnp.int32, shape, 1) < HEAD


def swap_halves(x):
    return pltpu.roll(x, HEAD, 1)


class RowGather:
    steps = 9

    def __init__(self, own, whole, send, recv):
        self.own, self.whole, self.send, self.recv = own, whole, send, recv
        sp, x, c = position()
        self.x, self.c = x, c
        self.right = (sp, lax.rem(x + 1, RING), c)
        self.left = (sp, lax.rem(x + RING - 1, RING), c)
        self.partner = (sp, x, 1 - c)
        self.half = own.shape[0] // 2

    def index(self, dx, other=False):
        return CORES * lax.rem(self.x + dx + RING, RING) + (1 - self.c if other else self.c)

    def slot(self, dx, other=False, part=None):
        ref = self.whole.at[self.index(dx, other)]
        return ref if part is None else ref.at[pl.ds(part * self.half, self.half)]

    def copy(self, k, src, dst, device):
        return remote(src, dst, self.send.at[k], self.recv.at[k], device)

    def out(self, k):
        if k == 0:
            return self.copy(0, self.own, self.slot(0), self.right)
        if k == 1:
            return self.copy(1, self.own, self.slot(0), self.left)
        if k == 2:
            return self.copy(2, self.own, self.slot(0), self.partner)
        if k == 3:
            return self.copy(3, self.slot(-1, part=0), self.slot(-1, part=0), self.right)
        if k == 4:
            return self.copy(4, self.slot(1, part=1), self.slot(1, part=1), self.left)
        if k == 5:
            return self.copy(5, self.slot(-1), self.slot(-1), self.partner)
        if k == 6:
            return self.copy(6, self.slot(1), self.slot(1), self.partner)
        if k == 7:
            return self.copy(7, self.slot(2, part=0), self.slot(2, part=0), self.partner)
        return self.copy(8, self.slot(2, part=1), self.slot(2, part=1), self.partner)

    def arrived(self, k):
        slots = (
            (-1, False, None),
            (1, False, None),
            (0, True, None),
            (2, False, 0),
            (2, False, 1),
            (-1, True, None),
            (1, True, None),
            (2, True, 0),
            (2, True, 1),
        )
        slot = self.slot(*slots[k])
        self.copy(k, slot, slot, self.partner).wait_recv()

    def start(self):
        for k in (0, 1, 2):
            self.out(k).start()

    def relay_near(self):
        self.arrived(0)
        self.out(3).start()
        self.out(5).start()
        self.arrived(1)
        self.out(4).start()
        self.out(6).start()

    def relay_far(self):
        self.arrived(3)
        self.out(7).start()
        self.arrived(4)
        self.out(8).start()

    def sent(self):
        for k in range(self.steps):
            self.out(k).wait_send()


def project_kernel(
    tok, gain, shift, taps, wa, wg, wq, wk, wv,
    conv_out, kvs, qs,
    whole, stacked, acc, squares, padded, tail, halo, weight_sem, send, recv, halo_send, halo_recv,
):
    sp, x, c = position()
    count = lax.axis_size("sp")
    rows, width = tok.shape
    local = wa.shape[1]
    loads = [
        pltpu.make_async_copy(w, stacked.at[:, pl.ds(local * i, local)], weight_sem.at[i])
        for i, w in enumerate((wa, wg, wq, wk, wv))
    ]
    for load in loads:
        load.start()
    later = (lax.rem(sp + 1, count), x, c)
    before = (lax.rem(sp + count - 1, count), x, c)
    net = RowGather(tok, whole, send, recv)
    greet([net.right, net.left, net.partner, later, before])
    net.start()
    for load in loads:
        load.wait()
    tile = 128

    def piece(ref, index, first=False):
        weights = stacked.at[pl.ds(pl.multiple_of(index * width, width), width)]

        @pl.loop(0, rows // tile)
        def _(i):
            here = pl.ds(pl.multiple_of(i * tile, tile), tile)
            wide = ref[here, :].astype(f32)
            scaled = (wide * gain[pl.ds(index, 1), :]).astype(bf16)
            total = jnp.dot(scaled, weights[...], preferred_element_type=f32)
            square = wide * wide
            square = square[:, : width // 2] + square[:, width // 2 :]
            if first:
                acc[here, :] = total
                squares[here, :] = square
            else:
                acc[here, :] += total
                squares[here, :] += square

    def gathered(dx, other=False):
        index = net.index(dx, other)
        piece(whole.at[index], index)

    piece(tok, net.index(0), first=True)
    net.arrived(2)
    gathered(0, True)
    net.relay_near()
    gathered(-1)
    gathered(1)
    net.arrived(5)
    gathered(-1, True)
    net.arrived(6)
    gathered(1, True)
    net.relay_far()
    gathered(2)
    net.arrived(7)
    net.arrived(8)
    gathered(2, True)

    model_width = width * RING * CORES

    @pl.loop(0, rows // tile)
    def _(i):
        here = pl.ds(pl.multiple_of(i * tile, tile), tile)
        scale = lax.rsqrt(jnp.sum(squares[here, :], axis=1, keepdims=True) / model_width + epsilon)
        projected = [
            (acc[here, pl.ds(local * k, local)] * scale).astype(bf16).astype(f32) for k in range(5)
        ]
        conv_a, conv_gate, query, key, value = projected
        padded[pl.ds(pl.multiple_of(32 + i * tile, 32), tile), :] = conv_a * jax.nn.sigmoid(conv_gate)
        low = left_lanes(query.shape)
        qs[0, here, :] = jnp.where(low, query, 0.0).astype(bf16)
        qs[1, here, :] = jnp.where(low, swap_halves(query), 0.0).astype(bf16)
        kvs[0, here, :] = jnp.where(low, key, swap_halves(value)).astype(bf16)
        kvs[1, here, :] = jnp.where(low, swap_halves(key), value).astype(bf16)

    tail[...] = padded[rows : rows + 32, :]
    shifts = shift[...].astype(f32)
    for head in range(2):
        lines = [shifts[head : head + 1, 128 * k : 128 * (k + 1)] for k in range(rows // 128)]
        lines.append(jnp.zeros((SHIFT_ROWS - len(lines), 128), f32))
        kvs[head, rows : rows + SHIFT_ROWS, :] = jnp.concatenate(lines, axis=0).astype(bf16)
    halo_copy = remote(tail, halo, halo_send, halo_recv, later)
    halo_copy.start()
    net.sent()
    halo_copy.wait()
    padded[0:32, :] = jnp.where(sp == 0, 0.0, halo[...])
    group = net.index(0)
    reach = taps.shape[0]
    tap_values = taps[:, pl.ds(pl.multiple_of(group * local, local), local)].astype(f32)
    step = 64

    @pl.loop(0, rows // step)
    def _(i):
        window = padded[pl.ds(pl.multiple_of(i * step, step), step + 32), :]
        total = jnp.zeros((step, local), f32)
        for rest in range(8):
            turned = window if rest == 0 else window[rest : rest + step + 24]
            for offset in range(rest, 33, 8):
                tap = offset - (33 - reach)
                if tap >= 0:
                    at = offset - rest
                    total = total + tap_values[tap : tap + 1, :] * turned[at : at + step]
        conv_out[pl.ds(pl.multiple_of(i * step, step), step), :] = total


def attention_kernel(
    kvs, qs, conv_own,
    attn_own, conv_all,
    kv_all, queries, sums, behinds, packed, returned,
    kv_send, kv_recv, q_send, q_recv, up_send, up_recv, down_send, down_recv,
    up_pass, up_passed, down_pass, down_passed, o_send, o_recv, x_send, x_recv,
):
    sp, x, c = position()
    z, y = sp // BLOCKS, lax.rem(sp, BLOCKS)
    rows = conv_own.shape[0]
    mirror = PLANES - 1 - z

    def at(plane, column, core):
        return (plane * BLOCKS + column, x, core)

    above, below = lax.rem(z + 1, PLANES), lax.rem(z + PLANES - 1, PLANES)
    partner = at(z, y, 1 - c)
    net = RowGather(conv_own, conv_all, x_send, x_recv)
    peers = [net.right, net.left, at(above, y, c), at(below, y, c)]
    for dy in range(BLOCKS):
        for dc in range(CORES):
            if dy or dc:
                peers.append(at(z, lax.rem(y + dy, BLOCKS), lax.rem(c + dc, CORES)))
            peers.append(at(mirror, dy, dc))
    greet(peers)

    def deliver(src, dst, send, recv, device, mine):
        @pl.when(mine)
        def _():
            pltpu.make_async_copy(src, dst, recv).start()

        @pl.when(jnp.logical_not(mine))
        def _():
            remote(src, dst, send, recv, device).start()

    def delivered(src, dst, send, recv, device, mine):
        @pl.when(jnp.logical_not(mine))
        def _():
            remote(src, dst, send, recv, device).wait_send()

    shipments = []
    for j in range(2):
        head = CORES * c + j
        for core in range(CORES):
            shipments.append((
                kvs.at[j], kv_all.at[z, y], kv_send.at[CORES * j + core], kv_recv.at[y],
                at(z, head, core), jnp.logical_and(head == y, c == core),
            ))
    q_plane = jnp.where(y < 2, z, mirror)
    q_core = jnp.where(jnp.logical_or(y == 0, y == BLOCKS - 1), 0, 1)
    q_slot = jnp.where(y < 2, 0, 1)
    for j in range(2):
        head = CORES * c + j
        shipments.append((
            qs.at[j], queries.at[q_slot], q_send.at[j], q_recv.at[q_slot],
            at(q_plane, head, q_core),
            jnp.logical_and(jnp.logical_and(y < 2, head == y), q_core == c),
        ))
    for shipment in shipments:
        deliver(*shipment)
    net.start()
    conv_all[net.index(0)] = conv_own[...]

    def landed(ref, sem):
        pltpu.make_async_copy(ref, ref, sem).wait()

    for block in range(BLOCKS):
        landed(kv_all.at[z, block], kv_recv.at[block])

    def half(plane):
        return kv_all.at[plane, pl.ds(CORES * c, CORES)]

    def other_half(plane):
        return kv_all.at[plane, pl.ds(CORES * (1 - c), CORES)]

    def up(step):
        plane = lax.rem(z - step + PLANES, PLANES)
        return remote(half(plane), half(plane), up_send.at[step], up_recv.at[step], at(above, y, c))

    def down(step):
        plane = lax.rem(z + step, PLANES)
        return remote(half(plane), half(plane), down_send.at[step], down_recv.at[step], at(below, y, c))

    def pass_up(step):
        plane = lax.rem(z - 1 - step + PLANES, PLANES)
        return remote(half(plane), half(plane), up_pass.at[step], up_passed.at[step], partner)

    def pass_down(step):
        plane = lax.rem(z + 1 + step, PLANES)
        return remote(half(plane), half(plane), down_pass.at[step], down_passed.at[step], partner)

    up(0).start()
    down(0).start()
    for slot in range(2):
        landed(queries.at[slot], q_recv.at[slot])

    row = lax.broadcasted_iota(jnp.int32, (256, 256), 0)
    column = lax.broadcasted_iota(jnp.int32, (256, 256), 1)
    later = jnp.where(row > column, 1.0, 0.0).astype(bf16)

    def block_step(which, plane, block, masked):
        shift_lines = kv_all[plane, block, rows : rows + SHIFT_ROWS, :].astype(f32)
        query = queries[which]
        for part in (1, 0):
            kv = kv_all[plane, block, 256 * part : 256 * (part + 1), :]
            shift = jnp.concatenate(
                [shift_lines[2 * part : 2 * part + 1], shift_lines[2 * part + 1 : 2 * part + 2]], axis=1
            )
            product = lax.dot_general(query, kv, (((1,), (1,)), ((), ())), preferred_element_type=f32)
            score = product * HEAD ** (-0.5) + shift
            fail = jnp.maximum(score, jnp.log(1.0 + jnp.exp(jnp.minimum(score, 80.0))))
            taken = score - fail
            if masked:
                query_row = lax.broadcasted_iota(jnp.int32, score.shape, 0)
                key_row = lax.broadcasted_iota(jnp.int32, score.shape, 1) + 256 * part
                allowed = key_row < query_row
                fail = jnp.where(allowed, fail, 0.0)
            rounded = fail.astype(bf16)
            between = jnp.dot(rounded, later, preferred_element_type=f32)
            behind = behinds[which, plane]
            weight = jnp.exp(taken - (between + jnp.concatenate([behind, behind], axis=1)))
            if masked:
                weight = jnp.where(allowed, weight, 0.0)
            sums[which, plane] += jnp.dot(weight.astype(bf16), kv, preferred_element_type=f32)
            total = between[:, 0:1] + rounded[:, 0:1].astype(f32)
            behinds[which, plane] = behind + jnp.broadcast_to(total, behind.shape)

    def attend(plane):
        @pl.loop(0, 2)
        def _(which):
            last = jnp.where(which == 0, z, mirror)
            block = jnp.where(which == 0, c, BLOCKS - 1 - c)

            @pl.when(plane <= last)
            def _():
                sums[which, plane] = jnp.zeros((rows, 128), f32)
                behinds[which, plane] = jnp.zeros((rows, 128), f32)

                @pl.when(plane == last)
                def _():
                    block_step(which, plane, block, True)

                first = jnp.where(plane == last, block, BLOCKS)

                @pl.loop(0, first)
                def _(i):
                    block_step(which, plane, first - 1 - i, False)

    up_steps, down_steps = PLANES // 2, PLANES // 2 - 1

    @pl.loop(0, up_steps + 1)
    def _(s):
        @pl.when(s > 0)
        def _():
            plane = lax.rem(z - s + PLANES, PLANES)
            landed(half(plane), up_recv.at[s - 1])

            @pl.when(s < up_steps)
            def _():
                up(s).start()

            pass_up(s - 1).start()

            @pl.when(s <= down_steps)
            def _():
                plane = lax.rem(z + s, PLANES)
                landed(half(plane), down_recv.at[s - 1])

                @pl.when(s < down_steps)
                def _():
                    down(s).start()

                pass_down(s - 1).start()

            landed(other_half(plane), up_passed.at[s - 1])

            @pl.when(s <= down_steps)
            def _():
                landed(other_half(lax.rem(z + s, PLANES)), down_passed.at[s - 1])

        @pl.when(s == 1)
        def _():
            net.relay_near()

        @pl.when(s == 2)
        def _():
            net.relay_far()

        @pl.loop(0, 2)
        def _(way):
            @pl.when(jnp.logical_or(way == 0, jnp.logical_and(s > 0, s <= down_steps)))
            def _():
                attend(lax.rem(jnp.where(way == 0, z - s, z + s) + PLANES, PLANES))

    for which in range(2):
        last = z if which == 0 else mirror

        @pl.loop(0, last)
        def _(i):
            plane = last - 1 - i
            behind = behinds[which, last]
            sums[which, last] += jnp.exp(-behind) * sums[which, plane]
            behinds[which, last] = behind + behinds[which, plane]

        done = sums[which, last]
        top, bottom = done[: rows // 2], done[rows // 2 :]
        packed[which] = jnp.where(left_lanes(top.shape), swap_halves(top), bottom).astype(bf16)

    for k in (2, 5, 6, 7, 8):
        net.arrived(k)
    net.sent()
    j = lax.rem(y, CORES)
    returns = []
    for which in range(2):
        owner = at(z, c, y // CORES) if which == 0 else at(mirror, BLOCKS - 1 - c, y // CORES)
        mine = jnp.logical_and(c == y, y // CORES == c) if which == 0 else None
        returns.append((packed.at[which], returned.at[j], o_send.at[which], o_recv.at[j], owner, mine))
    deliver(*returns[0])
    remote(*returns[1][:5]).start()
    for step in range(up_steps):
        up(step).wait_send()
        pass_up(step).wait_send()
    for step in range(down_steps):
        down(step).wait_send()
        pass_down(step).wait_send()
    for shipment in shipments:
        delivered(*shipment)
    for slot in range(2):
        landed(returned.at[slot], o_recv.at[slot])
    first, second = returned[0].astype(f32), returned[1].astype(f32)
    low = left_lanes(first.shape)
    attn_own[: rows // 2, :] = jnp.where(low, first, swap_halves(second)).astype(bf16)
    attn_own[rows // 2 :, :] = jnp.where(low, swap_halves(first), second).astype(bf16)
    delivered(*returns[0])
    remote(*returns[1][:5]).wait_send()


def mix_kernel(
    attn_own, conv_all, norm_gain, conv_gain, attn_gain, weights, mixed,
    whole, scaled, acc, squares, send, recv,
):
    rows, local = attn_own.shape
    pieces = conv_all.shape[0]
    channels = pieces * local
    net = RowGather(attn_own, whole, send, recv)
    greet([net.right, net.left, net.partner])
    net.start()
    tile = 64

    @pl.loop(0, rows // tile)
    def _(i):
        here = pl.ds(pl.multiple_of(i * tile, tile), tile)
        values = [conv_all[p, here, :] for p in range(pieces)]
        total = sum(values[1:], values[0])
        mean = jnp.sum(total, axis=1, keepdims=True) / channels
        centered = [v - mean for v in values]
        square = sum([v * v for v in centered[1:]], centered[0] * centered[0])
        spread = jnp.sum(square, axis=1, keepdims=True) / channels
        inverse = lax.rsqrt(spread + epsilon)
        power = jnp.zeros((tile, local), f32)
        for p in range(pieces):
            normed = centered[p] * inverse * norm_gain[p : p + 1, :]
            kept = (normed * jax.nn.sigmoid(normed)).astype(bf16).astype(f32)
            power = power + kept * kept
            scaled[here, local * p : local * (p + 1)] = (kept * conv_gain[p : p + 1, :]).astype(bf16)
        scale = lax.rsqrt(jnp.sum(power, axis=1, keepdims=True) / channels + epsilon)
        product = jnp.dot(scaled[here, :], weights[:channels, :], preferred_element_type=f32)
        acc[here, :] = product * scale

    def piece(ref, index, first=False):
        wide = ref[...].astype(f32)
        lanes = pl.ds(pl.multiple_of(index * local, local), local)
        scaled[:, lanes] = (wide * attn_gain[pl.ds(index, 1), :]).astype(bf16)
        if first:
            squares[...] = wide * wide
        else:
            squares[...] += wide * wide

    def gathered(dx, other=False):
        index = net.index(dx, other)
        piece(whole.at[index], index)

    piece(attn_own, net.index(0), first=True)
    net.arrived(2)
    gathered(0, True)
    net.relay_near()
    gathered(-1)
    gathered(1)
    net.arrived(5)
    gathered(-1, True)
    net.arrived(6)
    gathered(1, True)
    net.relay_far()
    gathered(2)
    net.arrived(7)
    net.arrived(8)
    gathered(2, True)
    net.sent()

    tile = 128

    @pl.loop(0, rows // tile)
    def _(i):
        here = pl.ds(pl.multiple_of(i * tile, tile), tile)
        scale = lax.rsqrt(jnp.sum(squares[here, :], axis=1, keepdims=True) / channels + epsilon)
        product = jnp.dot(scaled[here, :], weights[channels:, :], preferred_element_type=f32)
        mixed[here, :] = (acc[here, :] + product * scale).astype(bf16)


def in_vmem(count):
    return [pl.BlockSpec(memory_space=VMEM)] * count


def params(collective_id):
    return pltpu.CompilerParams(
        collective_id=collective_id, has_side_effects=True, vmem_limit_bytes=60 * 2**20
    )


def dma(*shape):
    return pltpu.SemaphoreType.DMA(shape)


def per_device(
    tokens, in_gain, conv_a_weight, conv_gate_weight, query_weight, key_weight, value_weight,
    conv_taps, conv_norm_gain, break_shift, conv_out_gain, attn_out_gain, out_weight,
):
    rows, width = tokens.shape
    local = conv_a_weight.shape[1]
    pieces = RING * CORES
    steps = RowGather.steps
    deep = rows + SHIFT_ROWS
    conv_own, kvs, qs = pl.pallas_call(
        project_kernel,
        name="project",
        out_shape=(
            jax.ShapeDtypeStruct((rows, local), f32),
            jax.ShapeDtypeStruct((2, deep, 128), bf16),
            jax.ShapeDtypeStruct((2, rows, 128), bf16),
        ),
        in_specs=in_vmem(4) + [pl.BlockSpec(memory_space=pl.ANY)] * 5,
        out_specs=tuple(in_vmem(3)),
        scratch_shapes=[
            VMEM((pieces, rows, width), bf16),
            VMEM((pieces * width, 5 * local), bf16),
            VMEM((rows, 5 * local), f32),
            VMEM((rows, local), f32),
            VMEM((rows + 32, local), f32),
            VMEM((32, local), f32),
            VMEM((32, local), f32),
            dma(5),
            dma(steps),
            dma(steps),
            pltpu.SemaphoreType.DMA,
            pltpu.SemaphoreType.DMA,
        ],
        compiler_params=params(0),
    )(
        tokens, in_gain.reshape(pieces, width), break_shift, conv_taps,
        conv_a_weight, conv_gate_weight, query_weight, key_weight, value_weight,
    )
    attn_own, conv_all = pl.pallas_call(
        attention_kernel,
        name="attention",
        out_shape=(
            jax.ShapeDtypeStruct((rows, local), bf16),
            jax.ShapeDtypeStruct((pieces, rows, local), f32),
        ),
        in_specs=in_vmem(3),
        out_specs=tuple(in_vmem(2)),
        scratch_shapes=[
            VMEM((PLANES, BLOCKS, deep, 128), bf16),
            VMEM((2, rows, 128), bf16),
            VMEM((2, PLANES, rows, 128), f32),
            VMEM((2, PLANES, rows, 128), f32),
            VMEM((2, rows // 2, 128), bf16),
            VMEM((2, rows // 2, 128), bf16),
            dma(4), dma(4), dma(2), dma(2), dma(4), dma(4), dma(3), dma(3),
            dma(4), dma(4), dma(3), dma(3), dma(2), dma(2), dma(steps), dma(steps),
        ],
        compiler_params=params(1),
    )(kvs, qs, conv_own)
    return pl.pallas_call(
        mix_kernel,
        name="mix",
        out_shape=jax.ShapeDtypeStruct((rows, out_weight.shape[1]), bf16),
        in_specs=in_vmem(6),
        out_specs=pl.BlockSpec(memory_space=VMEM),
        scratch_shapes=[
            VMEM((pieces, rows, local), bf16),
            VMEM((rows, pieces * local), bf16),
            VMEM((rows, out_weight.shape[1]), f32),
            VMEM((rows, local), f32),
            dma(steps),
            dma(steps),
        ],
        compiler_params=params(2),
    )(
        attn_own, conv_all, conv_norm_gain.reshape(pieces, local), conv_out_gain.reshape(pieces, local),
        attn_out_gain.reshape(pieces, local), out_weight,
    )


def solution(mesh):
    columns = P(None, ("fs", "tp"))
    return jax.shard_map(
        per_device,
        mesh=mesh,
        in_specs=(
            P("sp", ("fs", "tp")), P(), columns, columns, columns, columns, columns,
            P(), P(), P(("fs", "tp"), "sp"), P(), P(), columns,
        ),
        out_specs=P("sp", ("fs", "tp")),
        check_vma=False,
    )
```

time: 728 us -> 118 us (0.16)
  the two profiles are of different devices: /device:TPU:243 before, /device:TPU:91 now
where the time goes in v1:
time: 118 us; the launch traced here: 117 us
  Pallas kernels  114 us (97%)
  local copies, waits for them, and re-layouts  2.97 us (3%)
    pallas_call x1, Pallas kernels, per_device(): pl.pallas_call(attention_kernel, name='attention', out_shape=(jax.ShapeDt...  77.1 us
    pallas_call x1, Pallas kernels, per_device(): pl.pallas_call(project_kernel, name='project', out_shape=(jax.ShapeDtypeS...  22.2 us
    pallas_call x1, Pallas kernels, per_device(): pl.pallas_call(mix_kernel, name='mix', out_shape=jax.ShapeDtypeStruct((ro...  15 us

profile of v1, /device:TPU:91, one launch (start us, length us, event | category | flops | bytes accessed | tf_op | source)
XLA Modules:
  0.0 117.3 jit_solution(1325342130726103959)
XLA Ops:
  0.0 1.3 %reshape.12.gain = f32[8,256]{1,0:T(8,128)} reshape(f32[2048]{0:T(1024)} %param.14) | data formatting | bytes 16384 | tf_op jit(solution)/shard_map/reshape | solution.py:588
  1.3 22.2 %project.1 = (f32[512,128]{1,0:T(8,128)}, bf16[2,528,128]{2,1,0:T(8,128)(2,1)}, bf16[2,512,128]{2,1,0:T(8,128)(2,1)}) custom-call(bf16[512,256]{1,0:T(8,128)(2,1)} %tok.1, f32[8,256]{1,0:T(8,128)} %reshape.12.gain, bf16[2,512]{1,0:T(2,128)(2,1)} %shift.1, bf16[31,1024]{1,0:T(8,128)(2,1)} %taps.1, bf16[2048,128]{1,0:T(8,128)(2,1)} %wa.1, ...), custom_call_target="tpu_custom_call" | custom-call | tf_op jit(solution)/shard_map/project/pallas_call | solution.py:562
  23.5 77.1 %attention.1 = (bf16[512,128]{1,0:T(8,128)(2,1)}, f32[8,512,128]{2,1,0:T(8,128)}) custom-call(bf16[2,528,128]{2,1,0:T(8,128)(2,1)} %get-tuple-element.10.kvs, bf16[2,512,128]{2,1,0:T(8,128)(2,1)} %get-tuple-element.11.qs, f32[512,128]{1,0:T(8,128)} %get-tuple-element.12.conv_own), custom_call_target="tpu_custom_call" | custom-call | tf_op jit(solution)/shard_map/attention/pallas_call | solution.py:591
  100.7 15.0 %mix.1 = bf16[512,256]{1,0:T(8,128)(2,1)} custom-call(bf16[512,128]{1,0:T(8,128)(2,1)} %get-tuple-element.13.attn_own, f32[8,512,128]{2,1,0:T(8,128)} %get-tuple-element.14.conv_all, f32[8,128]{1,0:T(8,128)} %bitcast.3, f32[8,128]{1,0:T(8,128)} %bitcast.4, f32[8,128]{1,0:T(8,128)} %bitcast.5, bf16[2048,256]{1,0:T(8,128)(2,1)} %weights.1), custom_call_target="tpu_custom_call" | custom-call | tf_op jit(solution)/shard_map/mix/pallas_call | solution.py:612
  115.7 1.7 %copy.15 = bf16[512,256]{1,0:T(8,128)(2,1)} copy(bf16[512,256]{1,0:T(8,128)(2,1)} %mix.1) | data formatting | bytes 524288

commit v2 on v0

v2 whole, which is shorter than its diff:
```python
import jax
import jax.numpy as jnp
from jax import lax
from jax.experimental import pallas as pl
from jax.experimental.pallas import tpu as pltpu
from jax.sharding import PartitionSpec as P

MESH = pl.DeviceIdType.MESH
VMEM = pltpu.VMEM
HEAD = 64
PLANES, BLOCKS, RING, CORES = 8, 4, 4, 2
LOG2E = 1.4426950408889634
MESSAGES = 7
SHIFT_ROWS = 16
epsilon = 1e-06
f32, bf16 = jnp.float32, jnp.bfloat16


def position():
    return lax.axis_index("sp"), lax.axis_index("fs"), lax.axis_index("tp")


def greet(devices):
    barrier = pltpu.get_barrier_semaphore()
    for device in devices:
        pl.semaphore_signal(barrier, inc=1, device_id=device, device_id_type=MESH)
    pl.semaphore_wait(barrier, len(devices))


def remote(src, dst, send, recv, device):
    return pltpu.make_async_remote_copy(
        src_ref=src, dst_ref=dst, send_sem=send, recv_sem=recv, device_id=device, device_id_type=MESH
    )


def left_lanes(shape):
    return lax.broadcasted_iota(jnp.int32, shape, 1) < HEAD


def swap_halves(x):
    return pltpu.roll(x, HEAD, 1)


class RowGather:
    steps = 11

    def __init__(self, own, whole, send, recv):
        self.own, self.whole, self.send, self.recv = own, whole, send, recv
        sp, x, c = position()
        self.x, self.c = x, c
        self.right = (sp, lax.rem(x + 1, RING), c)
        self.left = (sp, lax.rem(x + RING - 1, RING), c)
        self.partner = (sp, x, 1 - c)
        self.half = own.shape[0] // 2

    def index(self, dx, other=False):
        return CORES * lax.rem(self.x + dx + RING, RING) + (1 - self.c if other else self.c)

    def slot(self, dx, other=False, part=None):
        return self.part(self.whole.at[self.index(dx, other)], part)

    def part(self, ref, part):
        return ref if part is None else ref.at[pl.ds(part * self.half, self.half)]

    def out(self, k):
        near = {0: (0, self.right), 1: (1, self.right), 2: (1, self.left), 3: (0, self.left), 4: (None, self.partner)}
        if k in near:
            part, device = near[k]
            src, dst = self.part(self.own, part), self.slot(0, part=part)
        else:
            dx, part, device = {
                5: (-1, 0, self.right),
                6: (1, 1, self.left),
                7: (-1, None, self.partner),
                8: (1, None, self.partner),
                9: (2, 0, self.partner),
                10: (2, 1, self.partner),
            }[k]
            src = dst = self.slot(dx, part=part)
        return remote(src, dst, self.send.at[k], self.recv.at[k], device)

    def arrived(self, *which):
        slots = (
            (-1, False, 0), (-1, False, 1), (1, False, 1), (1, False, 0), (0, True, None), (2, False, 0), (2, False, 1),
            (-1, True, None), (1, True, None), (2, True, 0), (2, True, 1),
        )
        for k in which:
            slot = self.slot(*slots[k])
            remote(slot, slot, self.send.at[k], self.recv.at[k], self.partner).wait_recv()

    def put(self, *which):
        for k in which:
            self.out(k).start()

    def start(self):
        self.put(0, 2, 1, 3, 4)

    def relay_first(self):
        self.arrived(0)
        self.put(5)
        self.arrived(2)
        self.put(6)

    def relay_near(self):
        self.arrived(1)
        self.put(7)
        self.arrived(3)
        self.put(8)

    def relay_far(self):
        self.arrived(5)
        self.put(9)
        self.arrived(6)
        self.put(10)

    def sent(self):
        for k in range(self.steps):
            self.out(k).wait_send()


def landed(ref, sem):
    pltpu.make_async_copy(ref, ref, sem).wait()


def layer_kernel(
    tok, gain, shift, taps, norm_gain, conv_gain, attn_gain, wa, wg, wq, wk, wv, wo,
    mixed,
    tokens_all, stacked, out_weights, acc, squares, padded, tail, halo, kvs, qs, conv_own, conv_all,
    kv_all, q_in, queries, sums, behinds, taken_a, taken_b, fail_a, fail_b, weight_a, weight_b,
    packed, returned, attn_own, attn_all, scaled, total,
    weight_sem, t_send, t_recv, h_send, h_recv, kv_send, kv_recv, pass_send, pass_recv, q_send, q_recv,
    up_send, up_recv, down_send, down_recv, up_pass, up_passed, down_pass, down_passed,
    o_send, o_recv, c_send, c_recv, a_send, a_recv,
):
    sp, x, c = position()
    count = lax.axis_size("sp")
    z, y = sp // BLOCKS, lax.rem(sp, BLOCKS)
    mirror = PLANES - 1 - z
    rows, width = tok.shape
    local = wa.shape[1]
    pieces = RING * CORES
    channels = pieces * local
    model_width = pieces * width

    def at(plane, column, core):
        return (plane * BLOCKS + column, x, core)

    loads = [
        pltpu.make_async_copy(w, stacked.at[:, pl.ds(local * i, local)], weight_sem.at[i])
        for i, w in enumerate((wa, wg, wq, wk, wv))
    ]
    loads.append(pltpu.make_async_copy(wo, out_weights, weight_sem.at[5]))
    for load in loads:
        load.start()

    above, below = lax.rem(z + 1, PLANES), lax.rem(z + PLANES - 1, PLANES)
    partner = at(z, y, 1 - c)
    later_rows = (lax.rem(sp + 1, count), x, c)
    earlier_rows = (lax.rem(sp + count - 1, count), x, c)
    net = RowGather(tok, tokens_all, t_send, t_recv)
    conv_net = RowGather(conv_own, conv_all, c_send, c_recv)
    attn_net = RowGather(attn_own, attn_all, a_send, a_recv)
    peers = [net.right, net.left, at(above, y, c), at(below, y, c), later_rows, earlier_rows]
    for dy in range(BLOCKS):
        for dc in range(CORES):
            if dy or dc:
                peers.append(at(z, lax.rem(y + dy, BLOCKS), lax.rem(c + dc, CORES)))
            peers.append(at(mirror, dy, dc))
    greet(peers)

    net.start()
    shifts = shift[...].astype(f32)
    for head in range(2):
        lines = [shifts[head : head + 1, 128 * k : 128 * (k + 1)] for k in range(rows // 128)]
        lines.append(jnp.zeros((SHIFT_ROWS - len(lines), 128), f32))
        kvs[head, rows : rows + SHIFT_ROWS, :] = jnp.concatenate(lines, axis=0).astype(bf16)
    for load in loads[:5]:
        load.wait()
    tile = 128

    def project(ref, index, first=False):
        weights = stacked.at[pl.ds(pl.multiple_of(index * width, width), width)]
        lines = gain[pl.ds(2 * index, 2), :]
        factor = jnp.concatenate([lines[0:1], lines[1:2]], axis=1)

        @pl.loop(0, rows // tile)
        def _(i):
            here = pl.ds(pl.multiple_of(i * tile, tile), tile)
            wide = ref[here, :].astype(f32)
            product = jnp.dot((wide * factor).astype(bf16), weights[...], preferred_element_type=f32)
            square = wide * wide
            square = square[:, : width // 2] + square[:, width // 2 :]
            if first:
                acc[here, :] = product
                squares[here, :] = square
            else:
                acc[here, :] += product
                squares[here, :] += square

    def project_slot(dx, other=False):
        index = net.index(dx, other)
        project(tokens_all.at[index], index)

    project(tok, net.index(0), first=True)
    net.arrived(4)
    project_slot(0, True)
    net.relay_first()
    net.relay_near()
    project_slot(-1)
    project_slot(1)
    net.arrived(7)
    project_slot(-1, True)
    net.arrived(8)
    project_slot(1, True)
    net.relay_far()
    project_slot(2)
    net.arrived(9, 10)
    project_slot(2, True)

    @pl.loop(0, rows // 2 // tile)
    def _(i):
        top = pl.ds(pl.multiple_of(i * tile, tile), tile)
        bottom = pl.ds(pl.multiple_of(rows // 2 + i * tile, tile), tile)
        query_halves = []
        for here in (top, bottom):
            scale = lax.rsqrt(jnp.sum(squares[here, :], axis=1, keepdims=True) / model_width + epsilon)
            conv_a, conv_gate, query, key, value = [
                (acc[here, pl.ds(local * k, local)] * scale).astype(bf16).astype(f32) for k in range(5)
            ]
            low = left_lanes(query.shape)
            query_halves.append(query)
            kvs[0, here, :] = jnp.where(low, key, swap_halves(value)).astype(bf16)
            kvs[1, here, :] = jnp.where(low, swap_halves(key), value).astype(bf16)
            inside = pl.ds(pl.multiple_of(32 + here.start, 32), tile)
            padded[inside, :] = conv_a * jax.nn.sigmoid(conv_gate)
        first, second = query_halves
        qs[0, top, :] = jnp.where(low, first, swap_halves(second)).astype(bf16)
        qs[1, top, :] = jnp.where(low, swap_halves(first), second).astype(bf16)

    tail[...] = padded[rows : rows + 32, :]

    def deliver(src, dst, send, recv, device, mine):
        @pl.when(mine)
        def _():
            pltpu.make_async_copy(src, dst, recv).start()

        @pl.when(jnp.logical_not(mine))
        def _():
            remote(src, dst, send, recv, device).start()

    def delivered(src, dst, send, recv, device, mine):
        @pl.when(jnp.logical_not(mine))
        def _():
            remote(src, dst, send, recv, device).wait_send()

    shipments = []
    for j in range(2):
        head = CORES * c + j
        shipments.append((
            kvs.at[j], kv_all.at[z, y], kv_send.at[j], kv_recv.at[lax.rem(y, CORES)],
            at(z, head, y // CORES), jnp.logical_and(head == y, y // CORES == c),
        ))
    q_plane = jnp.where(y < 2, z, mirror)
    q_core = jnp.where(jnp.logical_or(y == 0, y == BLOCKS - 1), 0, 1)
    q_slot = jnp.where(y < 2, 0, 1)
    for j in range(2):
        head = CORES * c + j
        shipments.append((
            qs.at[j], q_in.at[q_slot], q_send.at[j], q_recv.at[q_slot],
            at(q_plane, head, q_core),
            jnp.logical_and(jnp.logical_and(y < 2, head == y), q_core == c),
        ))
    for shipment in shipments:
        deliver(*shipment)
    halo_copy = remote(tail, halo, h_send, h_recv, later_rows)
    halo_copy.start()

    halo_copy.wait_recv()
    padded[0:32, :] = jnp.where(sp == 0, 0.0, halo[...])
    reach = taps.shape[0]
    tap_values = taps[:, pl.ds(pl.multiple_of(net.index(0) * local, local), local)].astype(f32)
    step = 64

    @pl.loop(0, rows // step)
    def _(i):
        window = padded[pl.ds(pl.multiple_of(i * step, step), step + 32), :]
        value = jnp.zeros((step, local), f32)
        for rest in range(8):
            turned = window if rest == 0 else window[rest : rest + step + 24]
            for offset in range(rest, 33, 8):
                tap = offset - (33 - reach)
                if tap >= 0:
                    start = offset - rest
                    value = value + tap_values[tap : tap + 1, :] * turned[start : start + step]
        here = pl.ds(pl.multiple_of(i * step, step), step)
        conv_own[here, :] = value
        conv_all[net.index(0), here, :] = value

    def ring_block(plane, parity):
        return kv_all.at[plane, CORES * c + parity]

    def passed_block(plane, parity):
        return kv_all.at[plane, CORES * (1 - c) + parity]

    def up_plane(k):
        return lax.rem(z - k + PLANES, PLANES)

    def down_plane(k):
        return lax.rem(z + k, PLANES)

    def up(m):
        block = ring_block(up_plane(m // 2), lax.rem(m, 2))
        return remote(block, block, up_send.at[m], up_recv.at[m], at(above, y, c))

    def down(m):
        block = ring_block(down_plane(m // 2), 1 - lax.rem(m, 2))
        return remote(block, block, down_send.at[m], down_recv.at[m], at(below, y, c))

    def pass_up(e):
        block = ring_block(up_plane(e // 2 + 1), lax.rem(e, 2))
        return remote(block, block, up_pass.at[e], up_passed.at[e], partner)

    def pass_down(e):
        block = ring_block(down_plane(e // 2 + 1), 1 - lax.rem(e, 2))
        return remote(block, block, down_pass.at[e], down_passed.at[e], partner)

    def pass_own(parity):
        block = ring_block(z, parity)
        return remote(block, block, pass_send.at[parity], pass_recv.at[parity], partner)

    landed(ring_block(z, 0), kv_recv.at[0])
    up(0).start()
    pass_own(0).start()
    landed(ring_block(z, 1), kv_recv.at[1])
    down(0).start()
    up(1).start()
    down(1).start()
    pass_own(1).start()
    conv_net.start()

    for which in range(2):
        @pl.loop(0, PLANES)
        def _(plane):
            sums[which, plane] = jnp.zeros((rows, 128), f32)
            behinds[which, plane] = jnp.zeros((rows, 128), f32)

        landed(q_in.at[which], q_recv.at[which])
        line = q_in[which].astype(f32)
        low = left_lanes(line.shape)
        queries[which, : rows // 2, :] = jnp.where(low, line, 0.0).astype(bf16)
        queries[which, rows // 2 :, :] = jnp.where(low, swap_halves(line), 0.0).astype(bf16)

    for parity in range(2):
        landed(passed_block(z, parity), pass_recv.at[parity])

    def event(e):
        landed(ring_block(up_plane(e // 2 + 1), lax.rem(e, 2)), up_recv.at[e])

        @pl.when(e + 2 < MESSAGES)
        def _():
            up(e + 2).start()

        pass_up(e).start()
        landed(ring_block(down_plane(e // 2 + 1), 1 - lax.rem(e, 2)), down_recv.at[e])

        @pl.when(e + 2 < MESSAGES)
        def _():
            down(e + 2).start()

        pass_down(e).start()
        for turn, relay in ((1, conv_net.relay_first), (2, conv_net.relay_near), (4, conv_net.relay_far)):
            pl.when(e == turn)(relay)

    def handed(e):
        landed(passed_block(up_plane(e // 2 + 1), lax.rem(e, 2)), up_passed.at[e])
        landed(passed_block(down_plane(e // 2 + 1), 1 - lax.rem(e, 2)), down_passed.at[e])

    row = lax.broadcasted_iota(jnp.int32, (256, 256), 0)
    column = lax.broadcasted_iota(jnp.int32, (256, 256), 1)
    later = jnp.where(row > column, 1.0, 0.0).astype(bf16)
    lasts, diagonals = (z, mirror), (c, BLOCKS - 1 - c)

    def score(which, plane, block, taken, fail, masked=False):
        lines = kv_all[plane, block, rows : rows + SHIFT_ROWS, :].astype(f32) * LOG2E
        line = jnp.concatenate([lines[k : k + 1] for k in range(rows // 128)], axis=1)
        product = lax.dot_general(
            queries[which], kv_all[plane, block, :rows, :], (((1,), (1,)), ((), ())), preferred_element_type=f32
        )
        value = product * (LOG2E * HEAD ** (-0.5)) + line
        lost = jnp.maximum(value, lax.log2(1.0 + jnp.exp2(jnp.minimum(value, 115.0))))
        kept = value - lost
        if masked:
            query_row = lax.broadcasted_iota(jnp.int32, value.shape, 0)
            allowed = lax.broadcasted_iota(jnp.int32, value.shape, 1) < query_row
            lost = jnp.where(allowed, lost, 0.0)
            kept = jnp.where(allowed, kept, -jnp.inf)
        taken[...] = kept
        fail[...] = lost.astype(bf16)

    def weigh(which, plane, taken, fail, weight):
        half = rows // 2
        near = jnp.dot(fail[:, half:], later, preferred_element_type=f32)
        far = jnp.dot(fail[:, :half], later, preferred_element_type=f32)
        behind = behinds[which, plane]
        near_total = near[:, 0:1] + fail[:, half : half + 1].astype(f32)
        far_total = far[:, 0:1] + fail[:, 0:1].astype(f32)
        behind_far = behind + jnp.broadcast_to(near_total, behind.shape)
        behinds[which, plane] = behind_far + jnp.broadcast_to(far_total, behind.shape)
        weight[:, half:] = jnp.exp2(taken[:, half:] - near - jnp.concatenate([behind, behind], axis=1)).astype(bf16)
        weight[:, :half] = jnp.exp2(
            taken[:, :half] - far - jnp.concatenate([behind_far, behind_far], axis=1)
        ).astype(bf16)

    def collect(which, plane, slot, block, weight):
        sums[which, slot] += jnp.dot(weight[...], kv_all[plane, block, :rows, :], preferred_element_type=f32)

    def diagonal(which):
        plane, block = lasts[which], diagonals[which]
        sums[which, PLANES] = jnp.zeros((rows, 128), f32)
        behinds[which, PLANES] = jnp.zeros((rows, 128), f32)
        score(which, plane, block, taken_a, fail_a, masked=True)
        weigh(which, PLANES, taken_a, fail_a, weight_a)
        collect(which, plane, PLANES, block, weight_a)

    segments = []
    for order in range(PLANES):
        k = (order + 1) // 2
        plane = up_plane(k) if order % 2 else down_plane(k)
        for which in range(2):
            whole = jnp.where(plane < lasts[which], BLOCKS, 0)
            segments.append((k, plane, which, jnp.where(plane == lasts[which], diagonals[which], whole)))

    def item(i):
        left, found = i, (jnp.int32(0), z, jnp.int32(0), jnp.int32(0))
        for k, plane, which, blocks in segments:
            inside = jnp.logical_and(left >= 0, left < blocks)
            here = (k, plane, which, blocks - 1 - left)
            found = tuple(jnp.where(inside, new, old) for new, old in zip(here, found))
            left = left - blocks
        return found

    items = (BLOCKS - 1) + BLOCKS * (PLANES - 1)

    def catch_up(done, target, handle):
        lax.fori_loop(done, target, lambda e, _: (handle(e), 0)[1], 0)
        return jnp.maximum(done, target)

    def prepare(i, step_needed, seen, had):
        needed = jnp.minimum(2 * step_needed, MESSAGES)
        expected = jnp.minimum(jnp.maximum(i - 1, 0) // 4, MESSAGES)
        seen = catch_up(seen, jnp.maximum(needed, expected), event)
        had = catch_up(had, needed, handed)
        return seen, had

    diagonal(0)
    zero = jnp.int32(0)
    first, second = item(zero), item(zero + 1)
    seen, had = prepare(zero, second[0], zero, zero)
    score(first[2], first[1], first[3], taken_a, fail_a)
    score(second[2], second[1], second[3], taken_b, fail_b)
    weigh(first[2], first[1], taken_a, fail_a, weight_a)

    def stages(now, after, coming, taken, fail, weight, other_taken, other_fail, other_weight):
        weigh(after[2], after[1], other_taken, other_fail, other_weight)
        score(coming[2], coming[1], coming[3], taken, fail)
        collect(now[2], now[1], now[1], now[3], weight)

    def pair(j, carried):
        now, after, seen, had = carried
        coming, following = item(2 * j + 2), item(2 * j + 3)
        seen, had = prepare(2 * j, jnp.maximum(coming[0], following[0]), seen, had)
        stages(now, after, coming, taken_a, fail_a, weight_a, taken_b, fail_b, weight_b)
        stages(after, coming, following, taken_b, fail_b, weight_b, taken_a, fail_a, weight_a)
        return coming, following, seen, had

    final, _, seen, had = lax.fori_loop(0, (items - 1) // 2, pair, (first, second, seen, had))
    collect(final[2], final[1], final[1], final[3], weight_a)
    seen = catch_up(seen, MESSAGES, event)
    catch_up(had, MESSAGES, handed)
    diagonal(1)

    for which in range(2):
        last = lasts[which]

        @pl.loop(0, last + 1)
        def _(i):
            plane = last - i
            behind = behinds[which, PLANES]
            sums[which, PLANES] += jnp.exp2(-behind) * sums[which, plane]
            behinds[which, PLANES] = behind + behinds[which, plane]

        done = sums[which, PLANES]
        top, bottom = done[: rows // 2], done[rows // 2 :]
        packed[which] = jnp.where(left_lanes(top.shape), swap_halves(top), bottom).astype(bf16)

    j = lax.rem(y, CORES)
    returns = []
    for which in range(2):
        owner = at(z, c, y // CORES) if which == 0 else at(mirror, BLOCKS - 1 - c, y // CORES)
        mine = jnp.logical_and(c == y, y // CORES == c) if which == 0 else None
        returns.append((packed.at[which], returned.at[j], o_send.at[which], o_recv.at[j], owner, mine))
    for e in range(MESSAGES):
        up(e).wait_send()
        pass_up(e).wait_send()
        down(e).wait_send()
        pass_down(e).wait_send()
    deliver(*returns[0])
    remote(*returns[1][:5]).start()
    net.sent()
    halo_copy.wait_send()
    for parity in range(2):
        pass_own(parity).wait_send()
    for shipment in shipments:
        delivered(*shipment)
    for slot in range(2):
        landed(returned.at[slot], o_recv.at[slot])
    first, second = returned[0].astype(f32), returned[1].astype(f32)
    low = left_lanes(first.shape)
    attn_own[: rows // 2, :] = jnp.where(low, first, swap_halves(second)).astype(bf16)
    attn_own[rows // 2 :, :] = jnp.where(low, swap_halves(first), second).astype(bf16)
    delivered(*returns[0])
    remote(*returns[1][:5]).wait_send()

    attn_net.start()
    conv_net.arrived(4, 7, 8, 9, 10)
    conv_net.sent()
    loads[5].wait()

    @pl.loop(0, rows // step)
    def _(i):
        here = pl.ds(pl.multiple_of(i * step, step), step)
        values = [conv_all[p, here, :] for p in range(pieces)]
        mean = jnp.sum(sum(values[1:], values[0]), axis=1, keepdims=True) / channels
        centered = [v - mean for v in values]
        square = sum([v * v for v in centered[1:]], centered[0] * centered[0])
        spread = jnp.sum(square, axis=1, keepdims=True) / channels
        inverse = lax.rsqrt(spread + epsilon)
        power = jnp.zeros((step, local), f32)
        for p in range(pieces):
            normed = centered[p] * inverse * norm_gain[p : p + 1, :]
            kept = (normed * jax.nn.sigmoid(normed)).astype(bf16).astype(f32)
            power = power + kept * kept
            scaled[here, local * p : local * (p + 1)] = (kept * conv_gain[p : p + 1, :]).astype(bf16)
        scale = lax.rsqrt(jnp.sum(power, axis=1, keepdims=True) / channels + epsilon)
        total[here, :] = jnp.dot(scaled[here, :], out_weights[:channels, :], preferred_element_type=f32) * scale

    def rescale(ref, index, first=False):
        wide = ref[...].astype(f32)
        lanes = pl.ds(pl.multiple_of(index * local, local), local)
        scaled[:, lanes] = (wide * attn_gain[pl.ds(index, 1), :]).astype(bf16)
        if first:
            squares[...] = wide * wide
        else:
            squares[...] += wide * wide

    def rescale_slot(dx, other=False):
        index = attn_net.index(dx, other)
        rescale(attn_all.at[index], index)

    rescale(attn_own, attn_net.index(0), first=True)
    attn_net.relay_first()
    attn_net.arrived(4)
    rescale_slot(0, True)
    attn_net.relay_near()
    rescale_slot(-1)
    rescale_slot(1)
    attn_net.arrived(7)
    rescale_slot(-1, True)
    attn_net.arrived(8)
    rescale_slot(1, True)
    attn_net.relay_far()
    rescale_slot(2)
    attn_net.arrived(9, 10)
    rescale_slot(2, True)

    @pl.loop(0, rows // tile)
    def _(i):
        here = pl.ds(pl.multiple_of(i * tile, tile), tile)
        scale = lax.rsqrt(jnp.sum(squares[here, :], axis=1, keepdims=True) / channels + epsilon)
        product = jnp.dot(scaled[here, :], out_weights[channels:, :], preferred_element_type=f32)
        mixed[here, :] = (total[here, :] + product * scale).astype(bf16)

    attn_net.sent()


def dma(*shape):
    return pltpu.SemaphoreType.DMA(shape)


def per_device(
    tokens, in_gain, conv_a_weight, conv_gate_weight, query_weight, key_weight, value_weight,
    conv_taps, conv_norm_gain, break_shift, conv_out_gain, attn_out_gain, out_weight,
):
    rows, width = tokens.shape
    local = conv_a_weight.shape[1]
    out_width = out_weight.shape[1]
    pieces = RING * CORES
    steps = RowGather.steps
    deep = rows + SHIFT_ROWS
    scratch = [
        VMEM((pieces, rows, width), bf16),
        VMEM((pieces * width, 5 * local), bf16),
        VMEM(out_weight.shape, bf16),
        VMEM((rows, 5 * local), f32),
        VMEM((rows, local), f32),
        VMEM((rows + 32, local), f32),
        VMEM((32, local), f32),
        VMEM((32, local), f32),
        VMEM((2, deep, 128), bf16),
        VMEM((2, rows // 2, 128), bf16),
        VMEM((rows, local), f32),
        VMEM((pieces, rows, local), f32),
        VMEM((PLANES, BLOCKS, deep, 128), bf16),
        VMEM((2, rows // 2, 128), bf16),
        VMEM((2, rows, 128), bf16),
        VMEM((2, PLANES + 1, rows, 128), f32),
        VMEM((2, PLANES + 1, rows, 128), f32),
        VMEM((rows, rows), f32),
        VMEM((rows, rows), f32),
        VMEM((rows, rows), bf16),
        VMEM((rows, rows), bf16),
        VMEM((rows, rows), bf16),
        VMEM((rows, rows), bf16),
        VMEM((2, rows // 2, 128), bf16),
        VMEM((2, rows // 2, 128), bf16),
        VMEM((rows, local), bf16),
        VMEM((pieces, rows, local), bf16),
        VMEM((rows, pieces * local), bf16),
        VMEM((rows, out_width), f32),
        dma(6), dma(steps), dma(steps), pltpu.SemaphoreType.DMA, pltpu.SemaphoreType.DMA,
        dma(2), dma(2), dma(2), dma(2), dma(2), dma(2),
        dma(MESSAGES), dma(MESSAGES), dma(MESSAGES), dma(MESSAGES),
        dma(MESSAGES), dma(MESSAGES), dma(MESSAGES), dma(MESSAGES),
        dma(2), dma(2), dma(steps), dma(steps), dma(steps), dma(steps),
    ]
    return pl.pallas_call(
        layer_kernel,
        name="layer",
        out_shape=jax.ShapeDtypeStruct((rows, out_width), bf16),
        in_specs=[pl.BlockSpec(memory_space=VMEM)] * 7 + [pl.BlockSpec(memory_space=pl.ANY)] * 6,
        out_specs=pl.BlockSpec(memory_space=VMEM),
        scratch_shapes=scratch,
        compiler_params=pltpu.CompilerParams(
            collective_id=0, has_side_effects=True, vmem_limit_bytes=60 * 2**20
        ),
    )(
        tokens, in_gain.reshape(2 * pieces, width // 2), break_shift, conv_taps,
        conv_norm_gain.reshape(pieces, local), conv_out_gain.reshape(pieces, local),
        attn_out_gain.reshape(pieces, local),
        conv_a_weight, conv_gate_weight, query_weight, key_weight, value_weight, out_weight,
    )


def solution(mesh):
    columns = P(None, ("fs", "tp"))
    return jax.shard_map(
        per_device,
        mesh=mesh,
        in_specs=(
            P("sp", ("fs", "tp")), P(), columns, columns, columns, columns, columns,
            P(), P(), P(("fs", "tp"), "sp"), P(), P(), columns,
        ),
        out_specs=P("sp", ("fs", "tp")),
        check_vma=False,
    )
```

time: 728 us -> 96.4 us (0.13)
  the two profiles are of different devices: /device:TPU:243 before, /device:TPU:121 now
where the time goes in v2:
time: 96.4 us; the launch traced here: 95.4 us
  Pallas kernels  93.7 us (97%)
  local copies, waits for them, and re-layouts  1.67 us (2%)
    pallas_call x1, Pallas kernels, per_device(): pl.pallas_call(layer_kernel, name='layer', out_shape=jax.ShapeDtypeStruct...  93.7 us

profile of v2, /device:TPU:121, one launch (start us, length us, event | category | flops | bytes accessed | tf_op | source)
XLA Modules:
  0.0 95.4 jit_solution(8309328654220531144)
XLA Ops:
  0.0 93.7 %layer.1 = bf16[512,256]{1,0:T(8,128)(2,1)} custom-call(bf16[512,256]{1,0:T(8,128)(2,1)} %tok.1, f32[16,128]{1,0:T(8,128)} %bitcast.4, bf16[2,512]{1,0:T(2,128)(2,1)} %shift.1, bf16[31,1024]{1,0:T(8,128)(2,1)} %taps.1, f32[8,128]{1,0:T(8,128)} %bitcast.5, f32[8,128]{1,0:T(8,128)} %bitcast.6, f32[8,128]{1,0:T(8,128)} %bitcast.7, bf16[2048,128]{1,0:T(8,128)(2,1)} %wa.1, ...), custom_call_target="tpu_custom_call" | custom-call | tf_op jit(solution)/shard_map/layer/pallas_call | solution.py:636
  93.8 1.7 %copy.15 = bf16[512,256]{1,0:T(8,128)(2,1)} copy(bf16[512,256]{1,0:T(8,128)(2,1)} %layer.1) | data formatting | bytes 524288

commit v3 on v2

--- a/solution.py
+++ b/solution.py
@@ -10,7 +10,8 @@
 HEAD = 64
 PLANES, BLOCKS, RING, CORES = 8, 4, 4, 2
 LOG2E = 1.4426950408889634
-MESSAGES = 7
+MESSAGES, NEAR = 8, 3
+HELP = 4
 SHIFT_ROWS = 16
 epsilon = 1e-06
 f32, bf16 = jnp.float32, jnp.bfloat16
@@ -127,10 +128,10 @@
     mixed,
     tokens_all, stacked, out_weights, acc, squares, padded, tail, halo, kvs, qs, conv_own, conv_all,
     kv_all, q_in, queries, sums, behinds, taken_a, taken_b, fail_a, fail_b, weight_a, weight_b,
-    packed, returned, attn_own, attn_all, scaled, total,
+    packed, far_packed, far_in, returned, attn_own, attn_all, scaled, total,
     weight_sem, t_send, t_recv, h_send, h_recv, kv_send, kv_recv, pass_send, pass_recv, q_send, q_recv,
     up_send, up_recv, down_send, down_recv, up_pass, up_passed, down_pass, down_passed,
-    o_send, o_recv, c_send, c_recv, a_send, a_recv,
+    f_send, f_recv, o_send, o_recv, c_send, c_recv, a_send, a_recv,
 ):
     sp, x, c = position()
     count = lax.axis_size("sp")
@@ -260,20 +261,28 @@
             kvs.at[j], kv_all.at[z, y], kv_send.at[j], kv_recv.at[lax.rem(y, CORES)],
             at(z, head, y // CORES), jnp.logical_and(head == y, y // CORES == c),
         ))
-    q_plane = jnp.where(y < 2, z, mirror)
     q_core = jnp.where(jnp.logical_or(y == 0, y == BLOCKS - 1), 0, 1)
     q_slot = jnp.where(y < 2, 0, 1)
+    helped, helping = z >= HELP, z < HELP
+    far_queries = []
     for j in range(2):
         head = CORES * c + j
         shipments.append((
             qs.at[j], q_in.at[q_slot], q_send.at[j], q_recv.at[q_slot],
-            at(q_plane, head, q_core),
-            jnp.logical_and(jnp.logical_and(y < 2, head == y), q_core == c),
+            at(z, head, q_core), jnp.logical_and(head == y, q_core == c),
+        ))
+        far_queries.append(remote(
+            qs.at[j], q_in.at[2 + q_slot], q_send.at[2 + j], q_recv.at[2 + q_slot], at(mirror, head, q_core)
         ))
     for shipment in shipments:
         deliver(*shipment)
     halo_copy = remote(tail, halo, h_send, h_recv, later_rows)
     halo_copy.start()
+
+    @pl.when(helped)
+    def _():
+        for copy in far_queries:
+            copy.start()
 
     halo_copy.wait_recv()
     padded[0:32, :] = jnp.where(sp == 0, 0.0, halo[...])
@@ -328,57 +337,89 @@
         block = ring_block(z, parity)
         return remote(block, block, pass_send.at[parity], pass_recv.at[parity], partner)
 
-    landed(ring_block(z, 0), kv_recv.at[0])
-    up(0).start()
-    pass_own(0).start()
-    landed(ring_block(z, 1), kv_recv.at[1])
-    down(0).start()
-    up(1).start()
-    down(1).start()
-    pass_own(1).start()
+    def rises(plane, k, core):
+        return jnp.logical_and(plane >= 0, jnp.logical_or(k < NEAR, core == 1))
+
+    def up_goes(m):
+        return jnp.logical_and(rises(z - m // 2, m // 2, c), z < PLANES - 1)
+
+    def up_comes(e, core):
+        return rises(z - 1 - e // 2, e // 2, core)
+
+    def down_goes(m):
+        return jnp.logical_and(jnp.logical_and(z + m // 2 < HELP, m < 2 * NEAR), z > 0)
+
+    def down_comes(e):
+        return jnp.logical_and(z + 1 + e // 2 < HELP, e < 2 * NEAR)
+
+    def send_up(m):
+        pl.when(up_goes(m))(lambda: up(m).start())
+
+    def send_down(m):
+        pl.when(down_goes(m))(lambda: down(m).start())
+
+    for parity in range(2):
+        landed(ring_block(z, parity), kv_recv.at[parity])
+        send_up(parity)
+        pass_own(parity).start()
+        if parity == 1:
+            send_down(0)
+            send_down(1)
     conv_net.start()
 
-    for which in range(2):
-        @pl.loop(0, PLANES)
-        def _(plane):
-            sums[which, plane] = jnp.zeros((rows, 128), f32)
-            behinds[which, plane] = jnp.zeros((rows, 128), f32)
-
-        landed(q_in.at[which], q_recv.at[which])
-        line = q_in[which].astype(f32)
+    @pl.loop(0, sums.shape[0])
+    def _(slot):
+        sums[slot] = jnp.zeros((rows, 128), f32)
+        behinds[slot] = jnp.zeros((rows, 128), f32)
+
+    def unpack(slot):
+        landed(q_in.at[slot], q_recv.at[slot])
+        line = q_in[slot].astype(f32)
         low = left_lanes(line.shape)
-        queries[which, : rows // 2, :] = jnp.where(low, line, 0.0).astype(bf16)
-        queries[which, rows // 2 :, :] = jnp.where(low, swap_halves(line), 0.0).astype(bf16)
-
+        queries[slot, : rows // 2, :] = jnp.where(low, line, 0.0).astype(bf16)
+        queries[slot, rows // 2 :, :] = jnp.where(low, swap_halves(line), 0.0).astype(bf16)
+
+    unpack(0)
+    unpack(1)
     for parity in range(2):
         landed(passed_block(z, parity), pass_recv.at[parity])
 
     def event(e):
-        landed(ring_block(up_plane(e // 2 + 1), lax.rem(e, 2)), up_recv.at[e])
-
-        @pl.when(e + 2 < MESSAGES)
+        @pl.when(up_comes(e, c))
         def _():
-            up(e + 2).start()
-
-        pass_up(e).start()
-        landed(ring_block(down_plane(e // 2 + 1), 1 - lax.rem(e, 2)), down_recv.at[e])
-
-        @pl.when(e + 2 < MESSAGES)
+            landed(ring_block(up_plane(e // 2 + 1), lax.rem(e, 2)), up_recv.at[e])
+
+            @pl.when(e + 2 < MESSAGES)
+            def _():
+                send_up(e + 2)
+
+            pass_up(e).start()
+
+        @pl.when(down_comes(e))
         def _():
-            down(e + 2).start()
-
-        pass_down(e).start()
+            landed(ring_block(down_plane(e // 2 + 1), 1 - lax.rem(e, 2)), down_recv.at[e])
+
+            @pl.when(e + 2 < 2 * NEAR)
+            def _():
+                send_down(e + 2)
+
+            pass_down(e).start()
+
         for turn, relay in ((1, conv_net.relay_first), (2, conv_net.relay_near), (4, conv_net.relay_far)):
             pl.when(e == turn)(relay)
 
     def handed(e):
-        landed(passed_block(up_plane(e // 2 + 1), lax.rem(e, 2)), up_passed.at[e])
-        landed(passed_block(down_plane(e // 2 + 1), 1 - lax.rem(e, 2)), down_passed.at[e])
+        @pl.when(up_comes(e, 1 - c))
+        def _():
+            landed(passed_block(up_plane(e // 2 + 1), lax.rem(e, 2)), up_passed.at[e])
+
+        @pl.when(down_comes(e))
+        def _():
+            landed(passed_block(down_plane(e // 2 + 1), 1 - lax.rem(e, 2)), down_passed.at[e])
 
     row = lax.broadcasted_iota(jnp.int32, (256, 256), 0)
     column = lax.broadcasted_iota(jnp.int32, (256, 256), 1)
     later = jnp.where(row > column, 1.0, 0.0).astype(bf16)
-    lasts, diagonals = (z, mirror), (c, BLOCKS - 1 - c)
 
     def score(which, plane, block, taken, fail, masked=False):
         lines = kv_all[plane, block, rows : rows + SHIFT_ROWS, :].astype(f32) * LOG2E
@@ -397,49 +438,82 @@
         taken[...] = kept
         fail[...] = lost.astype(bf16)
 
-    def weigh(which, plane, taken, fail, weight):
+    def weigh(slot, taken, fail, weight):
         half = rows // 2
         near = jnp.dot(fail[:, half:], later, preferred_element_type=f32)
         far = jnp.dot(fail[:, :half], later, preferred_element_type=f32)
-        behind = behinds[which, plane]
+        behind = behinds[slot]
         near_total = near[:, 0:1] + fail[:, half : half + 1].astype(f32)
         far_total = far[:, 0:1] + fail[:, 0:1].astype(f32)
         behind_far = behind + jnp.broadcast_to(near_total, behind.shape)
-        behinds[which, plane] = behind_far + jnp.broadcast_to(far_total, behind.shape)
+        behinds[slot] = behind_far + jnp.broadcast_to(far_total, behind.shape)
         weight[:, half:] = jnp.exp2(taken[:, half:] - near - jnp.concatenate([behind, behind], axis=1)).astype(bf16)
         weight[:, :half] = jnp.exp2(
             taken[:, :half] - far - jnp.concatenate([behind_far, behind_far], axis=1)
         ).astype(bf16)
 
-    def collect(which, plane, slot, block, weight):
-        sums[which, slot] += jnp.dot(weight[...], kv_all[plane, block, :rows, :], preferred_element_type=f32)
-
-    def diagonal(which):
-        plane, block = lasts[which], diagonals[which]
-        sums[which, PLANES] = jnp.zeros((rows, 128), f32)
-        behinds[which, PLANES] = jnp.zeros((rows, 128), f32)
-        score(which, plane, block, taken_a, fail_a, masked=True)
-        weigh(which, PLANES, taken_a, fail_a, weight_a)
-        collect(which, plane, PLANES, block, weight_a)
+    def collect(plane, slot, block, weight):
+        sums[slot] += jnp.dot(weight[...], kv_all[plane, block, :rows, :], preferred_element_type=f32)
 
     segments = []
-    for order in range(PLANES):
-        k = (order + 1) // 2
-        plane = up_plane(k) if order % 2 else down_plane(k)
-        for which in range(2):
-            whole = jnp.where(plane < lasts[which], BLOCKS, 0)
-            segments.append((k, plane, which, jnp.where(plane == lasts[which], diagonals[which], whole)))
+    for k in range(NEAR + 2):
+        for kind, plane in ((2, z - k), (2, z + k), (0, z - k)):
+            if kind and (k > NEAR or (k == 0 and segments)):
+                continue
+            if kind:
+                part = jnp.where(plane < HELP - 1 - z, BLOCKS, jnp.where(plane == HELP - 1 - z, BLOCKS // 2, 0))
+                blocks = jnp.where(jnp.logical_and(helping, plane >= 0), 2 * part, 0)
+            elif k == 0:
+                blocks = jnp.int32(BLOCKS - 1)
+            else:
+                blocks = jnp.where(plane >= 0, 2 * (BLOCKS if k <= NEAR else BLOCKS // 2), 0)
+            segments.append((jnp.int32(k), plane, jnp.int32(kind), blocks))
 
     def item(i):
-        left, found = i, (jnp.int32(0), z, jnp.int32(0), jnp.int32(0))
-        for k, plane, which, blocks in segments:
+        left, (k, plane, kind, place) = i, (jnp.int32(0), z, jnp.int32(0), jnp.int32(0))
+        for step_k, step_plane, step_kind, blocks in segments:
             inside = jnp.logical_and(left >= 0, left < blocks)
-            here = (k, plane, which, blocks - 1 - left)
-            found = tuple(jnp.where(inside, new, old) for new, old in zip(here, found))
+            k = jnp.where(inside, step_k, k)
+            plane = jnp.where(inside, step_plane, plane)
+            kind = jnp.where(inside, step_kind, kind)
+            place = jnp.where(inside, left, place)
             left = left - blocks
-        return found
+        mine, here = kind == 0, plane == z
+        part = jnp.where(plane < HELP - 1 - z, BLOCKS, BLOCKS // 2)
+        near_count = jnp.where(here, c, jnp.where(k <= NEAR, BLOCKS, BLOCKS // 2))
+        first_count = jnp.where(mine, near_count, part)
+        first_top = jnp.where(mine, jnp.where(here, c, BLOCKS), part)
+        second_top = jnp.where(mine, jnp.where(here, BLOCKS - 1 - c, BLOCKS), part)
+        second = place >= first_count
+        block = jnp.where(second, second_top - 1 - (place - first_count), first_top - 1 - place)
+        which = kind + jnp.where(second, 1, 0)
+        slot = jnp.where(mine, which, 2 + HELP * (which - 2) + plane)
+        return k, plane, which, block, slot
 
     items = (BLOCKS - 1) + BLOCKS * (PLANES - 1)
+    so_far, help_end = jnp.int32(0), jnp.int32(-BLOCKS)
+    for _, _, kind, blocks in segments:
+        so_far = so_far + blocks
+        help_end = jnp.where(jnp.logical_and(kind == 2, blocks > 0), so_far, help_end)
+
+    far_returns = [
+        remote(far_packed.at[w], far_in.at[w], f_send.at[w], f_recv.at[w], at(mirror, y, c)) for w in range(2)
+    ]
+
+    def pack(value):
+        top, bottom = value[: rows // 2], value[rows // 2 :]
+        return jnp.where(left_lanes(top.shape), swap_halves(top), bottom).astype(bf16)
+
+    def return_far():
+        for w in range(2):
+            base = 2 + HELP * w
+            for plane in range(HELP - 2, -1, -1):
+                behind = behinds[base + HELP - 1]
+                sums[base + HELP - 1] += jnp.exp2(-behind) * sums[base + plane]
+                behinds[base + HELP - 1] = behind + behinds[base + plane]
+            far_packed[w] = pack(sums[base + HELP - 1])
+        for copy in far_returns:
+            copy.start()
 
     def catch_up(done, target, handle):
         lax.fori_loop(done, target, lambda e, _: (handle(e), 0)[1], 0)
@@ -447,65 +521,89 @@
 
     def prepare(i, step_needed, seen, had):
         needed = jnp.minimum(2 * step_needed, MESSAGES)
-        expected = jnp.minimum(jnp.maximum(i - 1, 0) // 4, MESSAGES)
+        expected = jnp.minimum(jnp.maximum(i + 3, 0) // 4, MESSAGES)
         seen = catch_up(seen, jnp.maximum(needed, expected), event)
         had = catch_up(had, needed, handed)
         return seen, had
 
-    diagonal(0)
+    @pl.loop(0, 2)
+    def _(which):
+        block = jnp.where(which == 0, c, BLOCKS - 1 - c)
+        score(which, z, block, taken_a, fail_a, masked=True)
+        weigh(which, taken_a, fail_a, weight_a)
+        collect(z, which, block, weight_a)
+
+    @pl.when(helping)
+    def _():
+        unpack(2)
+        unpack(3)
+
     zero = jnp.int32(0)
     first, second = item(zero), item(zero + 1)
     seen, had = prepare(zero, second[0], zero, zero)
     score(first[2], first[1], first[3], taken_a, fail_a)
     score(second[2], second[1], second[3], taken_b, fail_b)
-    weigh(first[2], first[1], taken_a, fail_a, weight_a)
+    weigh(first[4], taken_a, fail_a, weight_a)
 
     def stages(now, after, coming, taken, fail, weight, other_taken, other_fail, other_weight):
-        weigh(after[2], after[1], other_taken, other_fail, other_weight)
+        weigh(after[4], other_taken, other_fail, other_weight)
         score(coming[2], coming[1], coming[3], taken, fail)
-        collect(now[2], now[1], now[1], now[3], weight)
+        collect(now[1], now[4], now[3], weight)
 
     def pair(j, carried):
         now, after, seen, had = carried
         coming, following = item(2 * j + 2), item(2 * j + 3)
         seen, had = prepare(2 * j, jnp.maximum(coming[0], following[0]), seen, had)
+        pl.when(jnp.logical_and(help_end > 2 * j - 2, help_end <= 2 * j))(return_far)
         stages(now, after, coming, taken_a, fail_a, weight_a, taken_b, fail_b, weight_b)
         stages(after, coming, following, taken_b, fail_b, weight_b, taken_a, fail_a, weight_a)
         return coming, following, seen, had
 
     final, _, seen, had = lax.fori_loop(0, (items - 1) // 2, pair, (first, second, seen, had))
-    collect(final[2], final[1], final[1], final[3], weight_a)
+    collect(final[1], final[4], final[3], weight_a)
+    pl.when(help_end > items - 3)(return_far)
     seen = catch_up(seen, MESSAGES, event)
     catch_up(had, MESSAGES, handed)
-    diagonal(1)
-
-    for which in range(2):
-        last = lasts[which]
-
-        @pl.loop(0, last + 1)
-        def _(i):
-            plane = last - i
-            behind = behinds[which, PLANES]
-            sums[which, PLANES] += jnp.exp2(-behind) * sums[which, plane]
-            behinds[which, PLANES] = behind + behinds[which, plane]
-
-        done = sums[which, PLANES]
-        top, bottom = done[: rows // 2], done[rows // 2 :]
-        packed[which] = jnp.where(left_lanes(top.shape), swap_halves(top), bottom).astype(bf16)
-
+
+    @pl.when(helped)
+    def _():
+        for w in range(2):
+            landed(far_in.at[w], f_recv.at[w])
+            line = far_in[w].astype(f32)
+            half = rows // 2
+            sums[w, :half] += jnp.exp2(-behinds[w, :half]) * swap_halves(line)
+            sums[w, half:] += jnp.exp2(-behinds[w, half:]) * line
+
+    for w in range(2):
+        packed[w] = pack(sums[w])
     j = lax.rem(y, CORES)
     returns = []
-    for which in range(2):
-        owner = at(z, c, y // CORES) if which == 0 else at(mirror, BLOCKS - 1 - c, y // CORES)
-        mine = jnp.logical_and(c == y, y // CORES == c) if which == 0 else None
-        returns.append((packed.at[which], returned.at[j], o_send.at[which], o_recv.at[j], owner, mine))
-    for e in range(MESSAGES):
-        up(e).wait_send()
-        pass_up(e).wait_send()
-        down(e).wait_send()
-        pass_down(e).wait_send()
-    deliver(*returns[0])
-    remote(*returns[1][:5]).start()
+    for w in range(2):
+        column = c if w == 0 else BLOCKS - 1 - c
+        returns.append((
+            packed.at[w], returned.at[j], o_send.at[w], o_recv.at[j], at(z, column, y // CORES),
+            jnp.logical_and(column == y, y // CORES == c),
+        ))
+    for back in returns:
+        deliver(*back)
+
+    @pl.loop(0, MESSAGES)
+    def _(e):
+        pl.when(up_goes(e))(lambda: up(e).wait_send())
+        pl.when(up_comes(e, c))(lambda: pass_up(e).wait_send())
+        pl.when(down_goes(e))(lambda: down(e).wait_send())
+        pl.when(down_comes(e))(lambda: pass_down(e).wait_send())
+
+    @pl.when(helping)
+    def _():
+        for copy in far_returns:
+            copy.wait_send()
+
+    @pl.when(helped)
+    def _():
+        for copy in far_queries:
+            copy.wait_send()
+
     net.sent()
     halo_copy.wait_send()
     for parity in range(2):
@@ -518,8 +616,8 @@
     low = left_lanes(first.shape)
     attn_own[: rows // 2, :] = jnp.where(low, first, swap_halves(second)).astype(bf16)
     attn_own[rows // 2 :, :] = jnp.where(low, swap_halves(first), second).astype(bf16)
-    delivered(*returns[0])
-    remote(*returns[1][:5]).wait_send()
+    for back in returns:
+        delivered(*back)
 
     attn_net.start()
     conv_net.arrived(4, 7, 8, 9, 10)
@@ -611,10 +709,10 @@
         VMEM((rows, local), f32),
         VMEM((pieces, rows, local), f32),
         VMEM((PLANES, BLOCKS, deep, 128), bf16),
-        VMEM((2, rows // 2, 128), bf16),
-        VMEM((2, rows, 128), bf16),
-        VMEM((2, PLANES + 1, rows, 128), f32),
-        VMEM((2, PLANES + 1, rows, 128), f32),
+        VMEM((4, rows // 2, 128), bf16),
+        VMEM((4, rows, 128), bf16),
+        VMEM((2 + 2 * HELP, rows, 128), f32),
+        VMEM((2 + 2 * HELP, rows, 128), f32),
         VMEM((rows, rows), f32),
         VMEM((rows, rows), f32),
         VMEM((rows, rows), bf16),
@@ -623,15 +721,17 @@
         VMEM((rows, rows), bf16),
         VMEM((2, rows // 2, 128), bf16),
         VMEM((2, rows // 2, 128), bf16),
+        VMEM((2, rows // 2, 128), bf16),
+        VMEM((2, rows // 2, 128), bf16),
         VMEM((rows, local), bf16),
         VMEM((pieces, rows, local), bf16),
         VMEM((rows, pieces * local), bf16),
         VMEM((rows, out_width), f32),
         dma(6), dma(steps), dma(steps), pltpu.SemaphoreType.DMA, pltpu.SemaphoreType.DMA,
-        dma(2), dma(2), dma(2), dma(2), dma(2), dma(2),
+        dma(2), dma(2), dma(2), dma(2), dma(4), dma(4),
         dma(MESSAGES), dma(MESSAGES), dma(MESSAGES), dma(MESSAGES),
         dma(MESSAGES), dma(MESSAGES), dma(MESSAGES), dma(MESSAGES),
-        dma(2), dma(2), dma(steps), dma(steps), dma(steps), dma(steps),
+        dma(2), dma(2), dma(2), dma(2), dma(steps), dma(steps), dma(steps), dma(steps),
     ]
     return pl.pallas_call(
         layer_kernel,

time: 96.4 us -> 88 us (0.913)
  Pallas kernels: 93.7 us -> 86.2 us
    pallas_call x1, Pallas kernels: 93.7 us -> 86.2 us  [per_device(): pl.pallas_call(layer_kernel, name='layer', out_shape=jax.ShapeDtypeStruct...]
where the time goes in v3:
time: 88 us; the launch traced here: 87.9 us
  Pallas kernels  86.2 us (98%)
  local copies, waits for them, and re-layouts  1.67 us (2%)
    pallas_call x1, Pallas kernels, per_device(): pl.pallas_call(layer_kernel, name='layer', out_shape=jax.ShapeDtypeStruct...  86.2 us

profile of v3, /device:TPU:121, one launch (start us, length us, event | category | flops | bytes accessed | tf_op | source)
XLA Modules:
  0.0 87.9 jit_solution(1191959776938929786)
XLA Ops:
  0.0 86.2 %layer.1 = bf16[512,256]{1,0:T(8,128)(2,1)} custom-call(bf16[512,256]{1,0:T(8,128)(2,1)} %tok.1, f32[16,128]{1,0:T(8,128)} %bitcast.4, bf16[2,512]{1,0:T(2,128)(2,1)} %shift.1, bf16[31,1024]{1,0:T(8,128)(2,1)} %taps.1, f32[8,128]{1,0:T(8,128)} %bitcast.5, f32[8,128]{1,0:T(8,128)} %bitcast.6, f32[8,128]{1,0:T(8,128)} %bitcast.7, bf16[2048,128]{1,0:T(8,128)(2,1)} %wa.1, ...), custom_call_target="tpu_custom_call" | custom-call | tf_op jit(solution)/shard_map/layer/pallas_call | solution.py:736
  86.2 1.7 %copy.15 = bf16[512,256]{1,0:T(8,128)(2,1)} copy(bf16[512,256]{1,0:T(8,128)(2,1)} %layer.1) | data formatting | bytes 524288

commit v4 on v3

--- a/solution.py
+++ b/solution.py
@@ -175,286 +175,7 @@
         lines = [shifts[head : head + 1, 128 * k : 128 * (k + 1)] for k in range(rows // 128)]
         lines.append(jnp.zeros((SHIFT_ROWS - len(lines), 128), f32))
         kvs[head, rows : rows + SHIFT_ROWS, :] = jnp.concatenate(lines, axis=0).astype(bf16)
-    for load in loads[:5]:
-        load.wait()
-    tile = 128
-
-    def project(ref, index, first=False):
-        weights = stacked.at[pl.ds(pl.multiple_of(index * width, width), width)]
-        lines = gain[pl.ds(2 * index, 2), :]
-        factor = jnp.concatenate([lines[0:1], lines[1:2]], axis=1)
-
-        @pl.loop(0, rows // tile)
-        def _(i):
-            here = pl.ds(pl.multiple_of(i * tile, tile), tile)
-            wide = ref[here, :].astype(f32)
-            product = jnp.dot((wide * factor).astype(bf16), weights[...], preferred_element_type=f32)
-            square = wide * wide
-            square = square[:, : width // 2] + square[:, width // 2 :]
-            if first:
-                acc[here, :] = product
-                squares[here, :] = square
-            else:
-                acc[here, :] += product
-                squares[here, :] += square
-
-    def project_slot(dx, other=False):
-        index = net.index(dx, other)
-        project(tokens_all.at[index], index)
-
-    project(tok, net.index(0), first=True)
-    net.arrived(4)
-    project_slot(0, True)
-    net.relay_first()
-    net.relay_near()
-    project_slot(-1)
-    project_slot(1)
-    net.arrived(7)
-    project_slot(-1, True)
-    net.arrived(8)
-    project_slot(1, True)
-    net.relay_far()
-    project_slot(2)
-    net.arrived(9, 10)
-    project_slot(2, True)
-
-    @pl.loop(0, rows // 2 // tile)
-    def _(i):
-        top = pl.ds(pl.multiple_of(i * tile, tile), tile)
-        bottom = pl.ds(pl.multiple_of(rows // 2 + i * tile, tile), tile)
-        query_halves = []
-        for here in (top, bottom):
-            scale = lax.rsqrt(jnp.sum(squares[here, :], axis=1, keepdims=True) / model_width + epsilon)
-            conv_a, conv_gate, query, key, value = [
-                (acc[here, pl.ds(local * k, local)] * scale).astype(bf16).astype(f32) for k in range(5)
-            ]
-            low = left_lanes(query.shape)
-            query_halves.append(query)
-            kvs[0, here, :] = jnp.where(low, key, swap_halves(value)).astype(bf16)
-            kvs[1, here, :] = jnp.where(low, swap_halves(key), value).astype(bf16)
-            inside = pl.ds(pl.multiple_of(32 + here.start, 32), tile)
-            padded[inside, :] = conv_a * jax.nn.sigmoid(conv_gate)
-        first, second = query_halves
-        qs[0, top, :] = jnp.where(low, first, swap_halves(second)).astype(bf16)
-        qs[1, top, :] = jnp.where(low, swap_halves(first), second).astype(bf16)
-
-    tail[...] = padded[rows : rows + 32, :]
-
-    def deliver(src, dst, send, recv, device, mine):
-        @pl.when(mine)
-        def _():
-            pltpu.make_async_copy(src, dst, recv).start()
-
-        @pl.when(jnp.logical_not(mine))
-        def _():
-            remote(src, dst, send, recv, device).start()
-
-    def delivered(src, dst, send, recv, device, mine):
-        @pl.when(jnp.logical_not(mine))
-        def _():
-            remote(src, dst, send, recv, device).wait_send()
-
-    shipments = []
-    for j in range(2):
-        head = CORES * c + j
-        shipments.append((
-            kvs.at[j], kv_all.at[z, y], kv_send.at[j], kv_recv.at[lax.rem(y, CORES)],
-            at(z, head, y // CORES), jnp.logical_and(head == y, y // CORES == c),
-        ))
-    q_core = jnp.where(jnp.logical_or(y == 0, y == BLOCKS - 1), 0, 1)
-    q_slot = jnp.where(y < 2, 0, 1)
     helped, helping = z >= HELP, z < HELP
-    far_queries = []
-    for j in range(2):
-        head = CORES * c + j
-        shipments.append((
-            qs.at[j], q_in.at[q_slot], q_send.at[j], q_recv.at[q_slot],
-            at(z, head, q_core), jnp.logical_and(head == y, q_core == c),
-        ))
-        far_queries.append(remote(
-            qs.at[j], q_in.at[2 + q_slot], q_send.at[2 + j], q_recv.at[2 + q_slot], at(mirror, head, q_core)
-        ))
-    for shipment in shipments:
-        deliver(*shipment)
-    halo_copy = remote(tail, halo, h_send, h_recv, later_rows)
-    halo_copy.start()
-
-    @pl.when(helped)
-    def _():
-        for copy in far_queries:
-            copy.start()
-
-    halo_copy.wait_recv()
-    padded[0:32, :] = jnp.where(sp == 0, 0.0, halo[...])
-    reach = taps.shape[0]
-    tap_values = taps[:, pl.ds(pl.multiple_of(net.index(0) * local, local), local)].astype(f32)
-    step = 64
-
-    @pl.loop(0, rows // step)
-    def _(i):
-        window = padded[pl.ds(pl.multiple_of(i * step, step), step + 32), :]
-        value = jnp.zeros((step, local), f32)
-        for rest in range(8):
-            turned = window if rest == 0 else window[rest : rest + step + 24]
-            for offset in range(rest, 33, 8):
-                tap = offset - (33 - reach)
-                if tap >= 0:
-                    start = offset - rest
-                    value = value + tap_values[tap : tap + 1, :] * turned[start : start + step]
-        here = pl.ds(pl.multiple_of(i * step, step), step)
-        conv_own[here, :] = value
-        conv_all[net.index(0), here, :] = value
-
-    def ring_block(plane, parity):
-        return kv_all.at[plane, CORES * c + parity]
-
-    def passed_block(plane, parity):
-        return kv_all.at[plane, CORES * (1 - c) + parity]
-
-    def up_plane(k):
-        return lax.rem(z - k + PLANES, PLANES)
-
-    def down_plane(k):
-        return lax.rem(z + k, PLANES)
-
-    def up(m):
-        block = ring_block(up_plane(m // 2), lax.rem(m, 2))
-        return remote(block, block, up_send.at[m], up_recv.at[m], at(above, y, c))
-
-    def down(m):
-        block = ring_block(down_plane(m // 2), 1 - lax.rem(m, 2))
-        return remote(block, block, down_send.at[m], down_recv.at[m], at(below, y, c))
-
-    def pass_up(e):
-        block = ring_block(up_plane(e // 2 + 1), lax.rem(e, 2))
-        return remote(block, block, up_pass.at[e], up_passed.at[e], partner)
-
-    def pass_down(e):
-        block = ring_block(down_plane(e // 2 + 1), 1 - lax.rem(e, 2))
-        return remote(block, block, down_pass.at[e], down_passed.at[e], partner)
-
-    def pass_own(parity):
-        block = ring_block(z, parity)
-        return remote(block, block, pass_send.at[parity], pass_recv.at[parity], partner)
-
-    def rises(plane, k, core):
-        return jnp.logical_and(plane >= 0, jnp.logical_or(k < NEAR, core == 1))
-
-    def up_goes(m):
-        return jnp.logical_and(rises(z - m // 2, m // 2, c), z < PLANES - 1)
-
-    def up_comes(e, core):
-        return rises(z - 1 - e // 2, e // 2, core)
-
-    def down_goes(m):
-        return jnp.logical_and(jnp.logical_and(z + m // 2 < HELP, m < 2 * NEAR), z > 0)
-
-    def down_comes(e):
-        return jnp.logical_and(z + 1 + e // 2 < HELP, e < 2 * NEAR)
-
-    def send_up(m):
-        pl.when(up_goes(m))(lambda: up(m).start())
-
-    def send_down(m):
-        pl.when(down_goes(m))(lambda: down(m).start())
-
-    for parity in range(2):
-        landed(ring_block(z, parity), kv_recv.at[parity])
-        send_up(parity)
-        pass_own(parity).start()
-        if parity == 1:
-            send_down(0)
-            send_down(1)
-    conv_net.start()
-
-    @pl.loop(0, sums.shape[0])
-    def _(slot):
-        sums[slot] = jnp.zeros((rows, 128), f32)
-        behinds[slot] = jnp.zeros((rows, 128), f32)
-
-    def unpack(slot):
-        landed(q_in.at[slot], q_recv.at[slot])
-        line = q_in[slot].astype(f32)
-        low = left_lanes(line.shape)
-        queries[slot, : rows // 2, :] = jnp.where(low, line, 0.0).astype(bf16)
-        queries[slot, rows // 2 :, :] = jnp.where(low, swap_halves(line), 0.0).astype(bf16)
-
-    unpack(0)
-    unpack(1)
-    for parity in range(2):
-        landed(passed_block(z, parity), pass_recv.at[parity])
-
-    def event(e):
-        @pl.when(up_comes(e, c))
-        def _():
-            landed(ring_block(up_plane(e // 2 + 1), lax.rem(e, 2)), up_recv.at[e])
-
-            @pl.when(e + 2 < MESSAGES)
-            def _():
-                send_up(e + 2)
-
-            pass_up(e).start()
-
-        @pl.when(down_comes(e))
-        def _():
-            landed(ring_block(down_plane(e // 2 + 1), 1 - lax.rem(e, 2)), down_recv.at[e])
-
-            @pl.when(e + 2 < 2 * NEAR)
-            def _():
-                send_down(e + 2)
-
-            pass_down(e).start()
-
-        for turn, relay in ((1, conv_net.relay_first), (2, conv_net.relay_near), (4, conv_net.relay_far)):
-            pl.when(e == turn)(relay)
-
-    def handed(e):
-        @pl.when(up_comes(e, 1 - c))
-        def _():
-            landed(passed_block(up_plane(e // 2 + 1), lax.rem(e, 2)), up_passed.at[e])
-
-        @pl.when(down_comes(e))
-        def _():
-            landed(passed_block(down_plane(e // 2 + 1), 1 - lax.rem(e, 2)), down_passed.at[e])
-
-    row = lax.broadcasted_iota(jnp.int32, (256, 256), 0)
-    column = lax.broadcasted_iota(jnp.int32, (256, 256), 1)
-    later = jnp.where(row > column, 1.0, 0.0).astype(bf16)
-
-    def score(which, plane, block, taken, fail, masked=False):
-        lines = kv_all[plane, block, rows : rows + SHIFT_ROWS, :].astype(f32) * LOG2E
-        line = jnp.concatenate([lines[k : k + 1] for k in range(rows // 128)], axis=1)
-        product = lax.dot_general(
-            queries[which], kv_all[plane, block, :rows, :], (((1,), (1,)), ((), ())), preferred_element_type=f32
-        )
-        value = product * (LOG2E * HEAD ** (-0.5)) + line
-        lost = jnp.maximum(value, lax.log2(1.0 + jnp.exp2(jnp.minimum(value, 115.0))))
-        kept = value - lost
-        if masked:
-            query_row = lax.broadcasted_iota(jnp.int32, value.shape, 0)
-            allowed = lax.broadcasted_iota(jnp.int32, value.shape, 1) < query_row
-            lost = jnp.where(allowed, lost, 0.0)
-            kept = jnp.where(allowed, kept, -jnp.inf)
-        taken[...] = kept
-        fail[...] = lost.astype(bf16)
-
-    def weigh(slot, taken, fail, weight):
-        half = rows // 2
-        near = jnp.dot(fail[:, half:], later, preferred_element_type=f32)
-        far = jnp.dot(fail[:, :half], later, preferred_element_type=f32)
-        behind = behinds[slot]
-        near_total = near[:, 0:1] + fail[:, half : half + 1].astype(f32)
-        far_total = far[:, 0:1] + fail[:, 0:1].astype(f32)
-        behind_far = behind + jnp.broadcast_to(near_total, behind.shape)
-        behinds[slot] = behind_far + jnp.broadcast_to(far_total, behind.shape)
-        weight[:, half:] = jnp.exp2(taken[:, half:] - near - jnp.concatenate([behind, behind], axis=1)).astype(bf16)
-        weight[:, :half] = jnp.exp2(
-            taken[:, :half] - far - jnp.concatenate([behind_far, behind_far], axis=1)
-        ).astype(bf16)
-
-    def collect(plane, slot, block, weight):
-        sums[slot] += jnp.dot(weight[...], kv_all[plane, block, :rows, :], preferred_element_type=f32)
-
     segments = []
     for k in range(NEAR + 2):
         for kind, plane in ((2, z - k), (2, z + k), (0, z - k)):
@@ -496,6 +217,290 @@
         so_far = so_far + blocks
         help_end = jnp.where(jnp.logical_and(kind == 2, blocks > 0), so_far, help_end)
 
+    for load in loads[:5]:
+        load.wait()
+    tile = 128
+
+    def project(ref, index, first=False):
+        weights = stacked.at[pl.ds(pl.multiple_of(index * width, width), width)]
+        lines = gain[pl.ds(2 * index, 2), :]
+        factor = jnp.concatenate([lines[0:1], lines[1:2]], axis=1)
+
+        @pl.loop(0, rows // 256)
+        def _(i):
+            here = pl.ds(pl.multiple_of(i * 256, 256), 256)
+            wide = ref[here, :].astype(f32)
+            product = jnp.dot((wide * factor).astype(bf16), weights[...], preferred_element_type=f32)
+            square = wide * wide
+            square = square[:, : width // 2] + square[:, width // 2 :]
+            if first:
+                acc[here, :] = product
+                squares[here, :] = square
+            else:
+                acc[here, :] += product
+                squares[here, :] += square
+
+    def project_slot(dx, other=False):
+        index = net.index(dx, other)
+        project(tokens_all.at[index], index)
+
+    project(tok, net.index(0), first=True)
+    net.arrived(4)
+    project_slot(0, True)
+    net.relay_first()
+    net.relay_near()
+    project_slot(-1)
+    project_slot(1)
+    net.arrived(7)
+    project_slot(-1, True)
+    net.arrived(8)
+    project_slot(1, True)
+    net.relay_far()
+    project_slot(2)
+    net.arrived(9, 10)
+    project_slot(2, True)
+
+    def projected(here, which):
+        scale = lax.rsqrt(jnp.sum(squares[here, :], axis=1, keepdims=True) / model_width + epsilon)
+        return [(acc[here, pl.ds(local * k, local)] * scale).astype(bf16).astype(f32) for k in which]
+
+    @pl.loop(0, rows // 2 // tile)
+    def _(i):
+        top = pl.ds(pl.multiple_of(i * tile, tile), tile)
+        bottom = pl.ds(pl.multiple_of(rows // 2 + i * tile, tile), tile)
+        query_halves = []
+        for here in (top, bottom):
+            query, key, value = projected(here, (2, 3, 4))
+            low = left_lanes(query.shape)
+            query_halves.append(query)
+            kvs[0, here, :] = jnp.where(low, key, swap_halves(value)).astype(bf16)
+            kvs[1, here, :] = jnp.where(low, swap_halves(key), value).astype(bf16)
+        first, second = query_halves
+        qs[0, top, :] = jnp.where(low, first, swap_halves(second)).astype(bf16)
+        qs[1, top, :] = jnp.where(low, swap_halves(first), second).astype(bf16)
+
+    def deliver(src, dst, send, recv, device, mine):
+        @pl.when(mine)
+        def _():
+            pltpu.make_async_copy(src, dst, recv).start()
+
+        @pl.when(jnp.logical_not(mine))
+        def _():
+            remote(src, dst, send, recv, device).start()
+
+    def delivered(src, dst, send, recv, device, mine):
+        @pl.when(jnp.logical_not(mine))
+        def _():
+            remote(src, dst, send, recv, device).wait_send()
+
+    shipments = []
+    for j in range(2):
+        head = CORES * c + j
+        shipments.append((
+            kvs.at[j], kv_all.at[z, y], kv_send.at[j], kv_recv.at[lax.rem(y, CORES)],
+            at(z, head, y // CORES), jnp.logical_and(head == y, y // CORES == c),
+        ))
+    q_core = jnp.where(jnp.logical_or(y == 0, y == BLOCKS - 1), 0, 1)
+    q_slot = jnp.where(y < 2, 0, 1)
+    far_queries = []
+    for j in range(2):
+        head = CORES * c + j
+        shipments.append((
+            qs.at[j], q_in.at[q_slot], q_send.at[j], q_recv.at[q_slot],
+            at(z, head, q_core), jnp.logical_and(head == y, q_core == c),
+        ))
+        far_queries.append(remote(
+            qs.at[j], q_in.at[2 + q_slot], q_send.at[2 + j], q_recv.at[2 + q_slot], at(mirror, head, q_core)
+        ))
+    for shipment in shipments:
+        deliver(*shipment)
+
+    @pl.when(helped)
+    def _():
+        for copy in far_queries:
+            copy.start()
+
+    @pl.loop(0, rows // tile)
+    def _(i):
+        here = pl.ds(pl.multiple_of(i * tile, tile), tile)
+        conv_a, conv_gate = projected(here, (0, 1))
+        padded[pl.ds(pl.multiple_of(32 + i * tile, 32), tile), :] = conv_a * jax.nn.sigmoid(conv_gate)
+
+    tail[...] = padded[rows : rows + 32, :]
+    halo_copy = remote(tail, halo, h_send, h_recv, later_rows)
+    halo_copy.start()
+
+    def ring_block(plane, parity):
+        return kv_all.at[plane, CORES * c + parity]
+
+    def passed_block(plane, parity):
+        return kv_all.at[plane, CORES * (1 - c) + parity]
+
+    def up_plane(k):
+        return lax.rem(z - k + PLANES, PLANES)
+
+    def down_plane(k):
+        return lax.rem(z + k, PLANES)
+
+    def up(m):
+        block = ring_block(up_plane(m // 2), lax.rem(m, 2))
+        return remote(block, block, up_send.at[m], up_recv.at[m], at(above, y, c))
+
+    def down(m):
+        block = ring_block(down_plane(m // 2), 1 - lax.rem(m, 2))
+        return remote(block, block, down_send.at[m], down_recv.at[m], at(below, y, c))
+
+    def pass_up(e):
+        block = ring_block(up_plane(e // 2 + 1), lax.rem(e, 2))
+        return remote(block, block, up_pass.at[e], up_passed.at[e], partner)
+
+    def pass_down(e):
+        block = ring_block(down_plane(e // 2 + 1), 1 - lax.rem(e, 2))
+        return remote(block, block, down_pass.at[e], down_passed.at[e], partner)
+
+    def pass_own(parity):
+        block = ring_block(z, parity)
+        return remote(block, block, pass_send.at[parity], pass_recv.at[parity], partner)
+
+    def rises(plane, k, core):
+        return jnp.logical_and(plane >= 0, jnp.logical_or(k < NEAR, core == 1))
+
+    def up_goes(m):
+        return jnp.logical_and(rises(z - m // 2, m // 2, c), z < PLANES - 1)
+
+    def up_comes(e, core):
+        return rises(z - 1 - e // 2, e // 2, core)
+
+    def down_goes(m):
+        return jnp.logical_and(jnp.logical_and(z + m // 2 < HELP, m < 2 * NEAR), z > 0)
+
+    def down_comes(e):
+        return jnp.logical_and(z + 1 + e // 2 < HELP, e < 2 * NEAR)
+
+    def send_up(m):
+        pl.when(up_goes(m))(lambda: up(m).start())
+
+    def send_down(m):
+        pl.when(down_goes(m))(lambda: down(m).start())
+
+    @pl.loop(0, sums.shape[0])
+    def _(slot):
+        sums[slot] = jnp.zeros((rows, 128), f32)
+        behinds[slot] = jnp.zeros((rows, 128), f32)
+
+    for parity in range(2):
+        landed(ring_block(z, parity), kv_recv.at[parity])
+        send_up(parity)
+        pass_own(parity).start()
+        if parity == 1:
+            send_down(0)
+            send_down(1)
+    halo_copy.wait_recv()
+    padded[0:32, :] = jnp.where(sp == 0, 0.0, halo[...])
+    reach = taps.shape[0]
+    tap_values = taps[:, pl.ds(pl.multiple_of(net.index(0) * local, local), local)].astype(f32)
+    step = 64
+
+    @pl.loop(0, rows // step)
+    def _(i):
+        window = padded[pl.ds(pl.multiple_of(i * step, step), step + 32), :]
+        value = jnp.zeros((step, local), f32)
+        for rest in range(8):
+            turned = window if rest == 0 else window[rest : rest + step + 24]
+            for offset in range(rest, 33, 8):
+                tap = offset - (33 - reach)
+                if tap >= 0:
+                    start = offset - rest
+                    value = value + tap_values[tap : tap + 1, :] * turned[start : start + step]
+        here = pl.ds(pl.multiple_of(i * step, step), step)
+        conv_own[here, :] = value
+        conv_all[net.index(0), here, :] = value
+
+    conv_net.start()
+
+    def unpack(slot):
+        landed(q_in.at[slot], q_recv.at[slot])
+        line = q_in[slot].astype(f32)
+        low = left_lanes(line.shape)
+        queries[slot, : rows // 2, :] = jnp.where(low, line, 0.0).astype(bf16)
+        queries[slot, rows // 2 :, :] = jnp.where(low, swap_halves(line), 0.0).astype(bf16)
+
+    unpack(0)
+    unpack(1)
+    for parity in range(2):
+        landed(passed_block(z, parity), pass_recv.at[parity])
+
+    def event(e):
+        @pl.when(up_comes(e, c))
+        def _():
+            landed(ring_block(up_plane(e // 2 + 1), lax.rem(e, 2)), up_recv.at[e])
+
+            @pl.when(e + 2 < MESSAGES)
+            def _():
+                send_up(e + 2)
+
+            pass_up(e).start()
+
+        @pl.when(down_comes(e))
+        def _():
+            landed(ring_block(down_plane(e // 2 + 1), 1 - lax.rem(e, 2)), down_recv.at[e])
+
+            @pl.when(e + 2 < 2 * NEAR)
+            def _():
+                send_down(e + 2)
+
+            pass_down(e).start()
+
+        for turn, relay in ((1, conv_net.relay_first), (2, conv_net.relay_near), (4, conv_net.relay_far)):
+            pl.when(e == turn)(relay)
+
+    def handed(e):
+        @pl.when(up_comes(e, 1 - c))
+        def _():
+            landed(passed_block(up_plane(e // 2 + 1), lax.rem(e, 2)), up_passed.at[e])
+
+        @pl.when(down_comes(e))
+        def _():
+            landed(passed_block(down_plane(e // 2 + 1), 1 - lax.rem(e, 2)), down_passed.at[e])
+
+    row = lax.broadcasted_iota(jnp.int32, (256, 256), 0)
+    column = lax.broadcasted_iota(jnp.int32, (256, 256), 1)
+    later = jnp.where(row > column, 1.0, 0.0).astype(bf16)
+
+    def score(which, plane, block, taken, fail, masked=False):
+        lines = kv_all[plane, block, rows : rows + SHIFT_ROWS, :].astype(f32) * LOG2E
+        line = jnp.concatenate([lines[k : k + 1] for k in range(rows // 128)], axis=1)
+        product = lax.dot_general(
+            queries[which], kv_all[plane, block, :rows, :], (((1,), (1,)), ((), ())), preferred_element_type=f32
+        )
+        value = product * (LOG2E * HEAD ** (-0.5)) + line
+        lost = jnp.maximum(value, lax.log2(1.0 + jnp.exp2(jnp.minimum(value, 115.0))))
+        kept = value - lost
+        if masked:
+            query_row = lax.broadcasted_iota(jnp.int32, value.shape, 0)
+            allowed = lax.broadcasted_iota(jnp.int32, value.shape, 1) < query_row
+            lost = jnp.where(allowed, lost, 0.0)
+            kept = jnp.where(allowed, kept, -jnp.inf)
+        taken[...] = kept
+        fail[...] = lost.astype(bf16)
+
+    def weigh(slot, taken, fail, weight):
+        half = rows // 2
+        near = jnp.dot(fail[:, half:], later, preferred_element_type=f32)
+        far = jnp.dot(fail[:, :half], later, preferred_element_type=f32)
+        behind = behinds[slot]
+        near_total = near[:, 0:1] + fail[:, half : half + 1].astype(f32)
+        far_total = far[:, 0:1] + fail[:, 0:1].astype(f32)
+        behind_far = behind + jnp.broadcast_to(near_total, behind.shape)
+        behinds[slot] = behind_far + jnp.broadcast_to(far_total, behind.shape)
+        weight[:, half:] = jnp.exp2(taken[:, half:] - near - jnp.concatenate([behind, behind], axis=1)).astype(bf16)
+        weight[:, :half] = jnp.exp2(
+            taken[:, :half] - far - jnp.concatenate([behind_far, behind_far], axis=1)
+        ).astype(bf16)
+
+    def collect(plane, slot, block, weight):
+        sums[slot] += jnp.dot(weight[...], kv_all[plane, block, :rows, :], preferred_element_type=f32)
+
     far_returns = [
         remote(far_packed.at[w], far_in.at[w], f_send.at[w], f_recv.at[w], at(mirror, y, c)) for w in range(2)
     ]
@@ -610,16 +615,6 @@
         pass_own(parity).wait_send()
     for shipment in shipments:
         delivered(*shipment)
-    for slot in range(2):
-        landed(returned.at[slot], o_recv.at[slot])
-    first, second = returned[0].astype(f32), returned[1].astype(f32)
-    low = left_lanes(first.shape)
-    attn_own[: rows // 2, :] = jnp.where(low, first, swap_halves(second)).astype(bf16)
-    attn_own[rows // 2 :, :] = jnp.where(low, swap_halves(first), second).astype(bf16)
-    for back in returns:
-        delivered(*back)
-
-    attn_net.start()
     conv_net.arrived(4, 7, 8, 9, 10)
     conv_net.sent()
     loads[5].wait()
@@ -642,6 +637,16 @@
         scale = lax.rsqrt(jnp.sum(power, axis=1, keepdims=True) / channels + epsilon)
         total[here, :] = jnp.dot(scaled[here, :], out_weights[:channels, :], preferred_element_type=f32) * scale
 
+    for slot in range(2):
+        landed(returned.at[slot], o_recv.at[slot])
+    first, second = returned[0].astype(f32), returned[1].astype(f32)
+    low = left_lanes(first.shape)
+    attn_own[: rows // 2, :] = jnp.where(low, first, swap_halves(second)).astype(bf16)
+    attn_own[rows // 2 :, :] = jnp.where(low, swap_halves(first), second).astype(bf16)
+    for back in returns:
+        delivered(*back)
+
+    attn_net.start()
     def rescale(ref, index, first=False):
         wide = ref[...].astype(f32)
         lanes = pl.ds(pl.multiple_of(index * local, local), local)

time: 88 us -> 84.1 us (0.956); the launches traced: 87.9 us -> 82.5 us
  Pallas kernels: 86.2 us -> 80.8 us
    pallas_call x1, Pallas kernels: 86.2 us -> 80.8 us  [per_device(): pl.pallas_call(layer_kernel, name='layer', out_shape=jax.ShapeDtypeStruct...]
where the time goes in v4:
time: 84.1 us; the launch traced here: 82.5 us
  Pallas kernels  80.8 us (96%)
  local copies, waits for them, and re-layouts  1.67 us (2%)
    pallas_call x1, Pallas kernels, per_device(): pl.pallas_call(layer_kernel, name='layer', out_shape=jax.ShapeDtypeStruct...  80.8 us

profile of v4, /device:TPU:121, one launch (start us, length us, event | category | flops | bytes accessed | tf_op | source)
XLA Modules:
  0.0 82.5 jit_solution(14185781633047597631)
XLA Ops:
  0.0 80.8 %layer.1 = bf16[512,256]{1,0:T(8,128)(2,1)} custom-call(bf16[512,256]{1,0:T(8,128)(2,1)} %tok.1, f32[16,128]{1,0:T(8,128)} %bitcast.4, bf16[2,512]{1,0:T(2,128)(2,1)} %shift.1, bf16[31,1024]{1,0:T(8,128)(2,1)} %taps.1, f32[8,128]{1,0:T(8,128)} %bitcast.5, f32[8,128]{1,0:T(8,128)} %bitcast.6, f32[8,128]{1,0:T(8,128)} %bitcast.7, bf16[2048,128]{1,0:T(8,128)(2,1)} %wa.1, ...), custom_call_target="tpu_custom_call" | custom-call | tf_op jit(solution)/shard_map/layer/pallas_call | solution.py:741
  80.8 1.7 %copy.15 = bf16[512,256]{1,0:T(8,128)(2,1)} copy(bf16[512,256]{1,0:T(8,128)(2,1)} %layer.1) | data formatting | bytes 524288

commit v5 on v4

--- a/solution.py
+++ b/solution.py
@@ -128,7 +128,7 @@
     mixed,
     tokens_all, stacked, out_weights, acc, squares, padded, tail, halo, kvs, qs, conv_own, conv_all,
     kv_all, q_in, queries, sums, behinds, taken_a, taken_b, fail_a, fail_b, weight_a, weight_b,
-    packed, far_packed, far_in, returned, attn_own, attn_all, scaled, total,
+    packed, far_packed, far_in, returned, attn_own, attn_all, scaled, total, norms,
     weight_sem, t_send, t_recv, h_send, h_recv, kv_send, kv_recv, pass_send, pass_recv, q_send, q_recv,
     up_send, up_recv, down_send, down_recv, up_pass, up_passed, down_pass, down_passed,
     f_send, f_recv, o_send, o_recv, c_send, c_recv, a_send, a_recv,
@@ -253,9 +253,9 @@
     project_slot(1)
     net.arrived(7)
     project_slot(-1, True)
+    net.relay_far()
     net.arrived(8)
     project_slot(1, True)
-    net.relay_far()
     project_slot(2)
     net.arrived(9, 10)
     project_slot(2, True)
@@ -635,7 +635,7 @@
             power = power + kept * kept
             scaled[here, local * p : local * (p + 1)] = (kept * conv_gain[p : p + 1, :]).astype(bf16)
         scale = lax.rsqrt(jnp.sum(power, axis=1, keepdims=True) / channels + epsilon)
-        total[here, :] = jnp.dot(scaled[here, :], out_weights[:channels, :], preferred_element_type=f32) * scale
+        norms[here, :] = jnp.broadcast_to(scale, (step, 128))
 
     for slot in range(2):
         landed(returned.at[slot], o_recv.at[slot])
@@ -647,6 +647,12 @@
         delivered(*back)
 
     attn_net.start()
+    @pl.loop(0, rows // 256)
+    def _(i):
+        here = pl.ds(pl.multiple_of(i * 256, 256), 256)
+        product = jnp.dot(scaled[here, :], out_weights[:channels, :], preferred_element_type=f32)
+        total[here, :] = product * jnp.concatenate([norms[here, :], norms[here, :]], axis=1)
+
     def rescale(ref, index, first=False):
         wide = ref[...].astype(f32)
         lanes = pl.ds(pl.multiple_of(index * local, local), local)
@@ -676,9 +682,9 @@
     attn_net.arrived(9, 10)
     rescale_slot(2, True)
 
-    @pl.loop(0, rows // tile)
+    @pl.loop(0, rows // 256)
     def _(i):
-        here = pl.ds(pl.multiple_of(i * tile, tile), tile)
+        here = pl.ds(pl.multiple_of(i * 256, 256), 256)
         scale = lax.rsqrt(jnp.sum(squares[here, :], axis=1, keepdims=True) / channels + epsilon)
         product = jnp.dot(scaled[here, :], out_weights[channels:, :], preferred_element_type=f32)
         mixed[here, :] = (total[here, :] + product * scale).astype(bf16)
@@ -732,6 +738,7 @@
         VMEM((pieces, rows, local), bf16),
         VMEM((rows, pieces * local), bf16),
         VMEM((rows, out_width), f32),
+        VMEM((rows, 128), f32),
         dma(6), dma(steps), dma(steps), pltpu.SemaphoreType.DMA, pltpu.SemaphoreType.DMA,
         dma(2), dma(2), dma(2), dma(2), dma(4), dma(4),
         dma(MESSAGES), dma(MESSAGES), dma(MESSAGES), dma(MESSAGES),

time: 84.1 us -> 82.8 us (0.985)
  Pallas kernels: 80.8 us -> 79.8 us
    pallas_call x1, Pallas kernels: 80.8 us -> 79.8 us  [per_device(): pl.pallas_call(layer_kernel, name='layer', out_shape=jax.ShapeDtypeStruct...]
where the time goes in v5:
time: 82.8 us; the launch traced here: 81.4 us
  Pallas kernels  79.8 us (96%)
  local copies, waits for them, and re-layouts  1.67 us (2%)
    pallas_call x1, Pallas kernels, per_device(): pl.pallas_call(layer_kernel, name='layer', out_shape=jax.ShapeDtypeStruct...  79.8 us
    unnamed x1, local copies, waits for them, and re-layouts  1.67 us

profile of v5, /device:TPU:121, one launch (start us, length us, event | category | flops | bytes accessed | tf_op | source)
XLA Modules:
  0.0 81.4 jit_solution(13508705618296687381)
XLA Ops:
  0.0 79.8 %layer.1 = bf16[512,256]{1,0:T(8,128)(2,1)} custom-call(bf16[512,256]{1,0:T(8,128)(2,1)} %tok.1, f32[16,128]{1,0:T(8,128)} %bitcast.4, bf16[2,512]{1,0:T(2,128)(2,1)} %shift.1, bf16[31,1024]{1,0:T(8,128)(2,1)} %taps.1, f32[8,128]{1,0:T(8,128)} %bitcast.5, f32[8,128]{1,0:T(8,128)} %bitcast.6, f32[8,128]{1,0:T(8,128)} %bitcast.7, bf16[2048,128]{1,0:T(8,128)(2,1)} %wa.1, ...), custom_call_target="tpu_custom_call" | custom-call | tf_op jit(solution)/shard_map/layer/pallas_call | solution.py:748
  79.8 1.7 %copy.15 = bf16[512,256]{1,0:T(8,128)(2,1)} copy(bf16[512,256]{1,0:T(8,128)(2,1)} %layer.1) | data formatting | bytes 524288
